TPU v7x, 128 devices: a whole 4x4x4 slice. The times are simulated.
128 devices in a mesh: rep: 2 (over z_hi), fs: 32 (over z_lo, y, x), tp: 2 (over core).
Axes of the slice: x: 4, y: 4, z: 4 (z_hi: 2, z_lo: 2; z = z_hi * 2 + z_lo), core: 2. Of those that a mesh axis runs over, the one named last changes fastest.
Arguments:
- tokens: bfloat16 [64, 512, 2048], P(('rep', 'fs'), 'tp'), may hold values from -6 to 6
- norm_first: bfloat16 [2048], replicated, may hold values from 0.099609375 to 1.8984375
- norm_mixer: bfloat16 [2048], replicated, may hold values from 0.099609375 to 1.8984375
- norm_second: bfloat16 [2048], replicated, may hold values from 0.099609375 to 1.8984375
- ffn_gate: bfloat16 [2048, 2816], P('fs', 'tp'), may hold values from -0.125 to 0.125
- ffn_up: bfloat16 [2048, 2816], P('fs', 'tp'), may hold values from -0.125 to 0.125
- ffn_down: bfloat16 [2816, 2048], P('tp', 'fs'), may hold values from -0.109375 to 0.109375
- conv_value: bfloat16 [2048, 512], P('fs', 'tp'), may hold values from -0.125 to 0.125
- conv_gate: bfloat16 [2048, 512], P('fs', 'tp'), may hold values from -0.125 to 0.125
- depthwise: bfloat16 [31, 512], P(None, 'tp'), may hold values from -1.5 to 1.5
- conv_gain: bfloat16 [512], P('tp'), may hold values from 0.099609375 to 1.8984375
- conv_out: bfloat16 [512, 2048], P('tp', 'fs'), may hold values from -0.25 to 0.25
Outputs:
- mixed: bfloat16 [64, 512, 2048], P(('rep', 'fs'), 'tp')
All inputs are finite; a program needn't handle non-finite values.
Results may differ from a plain program's by a relative error of at most 0.0095.
Values may be sent and summed in bfloat16 or wider, within the bound.
No kernel may reach another device: no remote copies, remote signals or barrier semaphores. Data moves between devices by JAX's collectives and lax.ppermute only.
A program may use at most 128 MiB of HBM per device.

v0:
```python
import jax
import jax.numpy as jnp
from jax import lax
from jax.sharding import PartitionSpec as P

ROW_EPS = 0.05
CHAN_EPS = 0.02


def sent_to_all(x, axis):
    copies = jnp.broadcast_to(x, (lax.axis_size(axis), *x.shape))
    return lax.all_to_all(copies, axis, split_axis=0, concat_axis=0, tiled=True)


def laid_out(pieces, dim):
    lengths = list(pieces.shape[1:])
    lengths[dim] *= pieces.shape[0]
    return jnp.moveaxis(pieces, 0, dim).reshape(lengths)


def collect(x, axis, dim):
    pieces = sent_to_all(x, axis)
    return laid_out(pieces, dim)


def split_up(x, dim, count):
    lengths = x.shape
    pieces = x.reshape(*lengths[:dim], count, lengths[dim] // count, *lengths[dim + 1 :])
    return jnp.moveaxis(pieces, dim, 0)


def sent_and_summed(x, axis, dim):
    count = lax.axis_size(axis)
    pieces = lax.all_to_all(split_up(x, dim, count), axis, 0, 0, tiled=True)
    return jnp.sum(pieces.astype(jnp.float32), axis=0)


def rows_first(arrays, axis, dims):
    turned = [jnp.moveaxis(a, dim, 0) for a, dim in zip(arrays, dims)]
    both = jnp.concatenate([t.reshape(len(t), -1) for t in turned], axis=1)
    filled, at, finished = (lax.all_gather(both, axis, axis=0, tiled=True), 0, [])
    for t, dim in zip(turned, dims):
        section = filled[:, at : at + t[0].size].reshape(-1, *t.shape[1:])
        finished.append(jnp.moveaxis(section, 0, dim))
        at += t[0].size
    return tuple(finished)


def in_one_piece(arrays, axis, dim, along):
    widths = [a.shape[along] for a in arrays]
    both = jnp.concatenate(arrays, axis=along)
    filled = lax.all_gather(both, axis, axis=dim, tiled=True)
    return tuple(jnp.split(filled, [sum(widths[:k]) for k in range(1, len(widths))], axis=along))


def over_pieces(x, axis):
    return lax.all_gather(x, axis).sum(0)


def rms_rows(stream, gain_vec):
    square_mean = jnp.mean(stream * stream, axis=-1, keepdims=True)
    return (stream * lax.rsqrt(square_mean + ROW_EPS) * gain_vec.astype(jnp.float32)).astype(
        jnp.bfloat16
    )


def widen(normed):
    return collect(normed, "tp", 0)


def narrow(partial_value):
    return sent_and_summed(partial_value.astype(jnp.bfloat16), "tp", 0)


def add_pair(gathered, portions):
    return (
        jnp.dot(gathered, portions[0], preferred_element_type=jnp.float32),
        jnp.dot(gathered, portions[1], preferred_element_type=jnp.float32),
    )


def hidden_units(gathered, whole_gate, whole_up):
    gate_rows = jnp.dot(gathered, whole_gate, preferred_element_type=jnp.float32)
    up_rows = jnp.dot(gathered, whole_up, preferred_element_type=jnp.float32)
    return (jax.nn.silu(gate_rows) * up_rows).astype(jnp.bfloat16)


def causal_taps(glu, kernel):
    length = glu.shape[0]
    taps = kernel.shape[0]
    padded = jnp.pad(glu, ((taps - 1, 0), (0, 0)))
    output = jnp.zeros_like(glu)
    for tap_index in range(taps):
        output = output + padded[tap_index : tap_index + length] * kernel[tap_index]
    return output


def shards(
    tokens,
    norm_first,
    norm_mixer,
    norm_second,
    ffn_gate,
    ffn_up,
    ffn_down,
    conv_value,
    conv_gate,
    depthwise,
    conv_gain,
    conv_out,
):
    width = tokens.shape[-1]
    stream = tokens.reshape(-1, width).astype(jnp.float32)
    first_rows = widen(rms_rows(stream, norm_first))
    whole_gate, whole_up, whole_down = rows_first((ffn_gate, ffn_up, ffn_down), "fs", (0, 0, 1))
    hidden = hidden_units(first_rows, whole_gate, whole_up)
    first_out = jnp.dot(hidden, whole_down, preferred_element_type=jnp.float32)
    stream = stream + 0.5 * narrow(first_out)
    gathered = widen(rms_rows(stream, norm_mixer))
    values, gates = add_pair(gathered, in_one_piece((conv_value, conv_gate), "fs", 0, 1))
    glu = values * jax.nn.sigmoid(gates)
    conv = causal_taps(glu, depthwise.astype(jnp.float32))
    channels = conv.shape[1] * lax.axis_size("tp")
    average = over_pieces(jnp.sum(conv, axis=1), "tp") / channels
    centred = conv - average[:, None]
    spread = over_pieces(jnp.sum(centred * centred, axis=1), "tp") / channels
    activated = jax.nn.silu(
        centred * lax.rsqrt(spread[:, None] + CHAN_EPS) * conv_gain.astype(jnp.float32)
    ).astype(jnp.bfloat16)
    stream = stream + narrow(
        jnp.dot(activated, collect(conv_out, "fs", 1), preferred_element_type=jnp.float32)
    )
    second_rows = widen(rms_rows(stream, norm_second))
    second_hidden = hidden_units(second_rows, whole_gate, whole_up)
    second_out = jnp.dot(second_hidden, whole_down, preferred_element_type=jnp.float32)
    stream = stream + 0.5 * narrow(second_out)
    return stream.astype(jnp.bfloat16).reshape(tokens.shape)


def solution(mesh):
    in_specs = (
        P(("rep", "fs"), "tp", None),
        P(),
        P(),
        P(),
        P("fs", "tp"),
        P("fs", "tp"),
        P("tp", "fs"),
        P("fs", "tp"),
        P("fs", "tp"),
        P(None, "tp"),
        P("tp"),
        P("tp", "fs"),
    )
    out_specs = P(("rep", "fs"), "tp", None)
    return jax.shard_map(shards, mesh=mesh, in_specs=in_specs, out_specs=out_specs, check_vma=False)
```

profile of v0, /device:TPU:3, one launch (start us, length us, event | category | flops | bytes accessed | tf_op | source)
XLA Modules:
  0.0 431.1 jit_solution(4163618448635915298)
XLA Ops:
  6.5 2.0 pad_maximum_fusion
  8.6 0.7 convert_element_type.69
  9.9 1.6 broadcast_in_dim.8
  11.5 4.6 %all-to-all-start = ((bf16[2,256,2048]{2,1,0:T(8,128)(2,1)}), bf16[2,256,2048]{2,1,0:T(8,128)(2,1)S(1)}, u32[]{:S(2)}, u32[]{:S(2)}) async-start(bf16[2,256,2048]{2,1,0:T(8,128)(2,1)} %broadcast_in_dim.8), calls=%async_computation | async-start | bytes 4194304 | tf_op jit(solution)/shard_map/all_to_all | solution.py:12
  16.1 0.6 pad_maximum_fusion.1
  17.0 1.6 all-to-all-done
  18.6 185.9 %all-gather.7.cloned.1.call-done = bf16[2048,4224]{1,0:T(8,128)(2,1)} async-done(((bf16[64,4224]{1,0:T(8,128)(2,1)}), bf16[2048,4224]{1,0:T(8,128)(2,1)}) %all-gather.7.cloned.1.call-update) | async-done | bytes 17301520 | tf_op jit(solution)/shard_map/all_gather | solution.py:41
  204.5 7.6 %fusion.10 = f32[512,1408]{1,0:T(8,128)} fusion(bf16[512,2048]{1,0:T(8,128)(2,1)S(1)} %bitcast.80, bf16[2048,4224]{1,0:T(8,128)(2,1)} %all-gather.7.cloned.1.call-done), kind=kOutput, calls=%fused_computation.10 | convolution fusion | flops 2952790016 | bytes 10747904 | tf_op jit(solution)/shard_map/dot_general | solution.py:83
  212.1 13.3 %fusion.24 = bf16[512,2048]{1,0:T(8,128)(2,1)} fusion(bf16[2048,4224]{1,0:T(8,128)(2,1)} %all-gather.7.cloned.1.call-done, bf16[512,2048]{1,0:T(8,128)(2,1)S(1)} %bitcast.81, f32[512,1408]{1,0:T(8,128)} %fusion.10), kind=kOutput, calls=%fused_computation.20 | convolution fusion | flops 5910953984 | bytes 18612224 | tf_op jit(solution)/shard_map/dot_general | solution.py:117
  225.3 7.5 %all_to_all.35 = bf16[2,256,2048]{2,1,0:T(8,128)(2,1)S(1)} all-to-all(bf16[2,256,2048]{2,1,0:T(8,128)(2,1)} %bitcast.88), channel_id=1, replica_groups=mesh['rep'=2,'fs'=32,'tp'=2] {'tp'}, dimensions={0} | all-to-all | bytes 4194304 | tf_op jit(solution)/shard_map/all_to_all | solution.py:34
  234.4 6.3 %all_to_all.36 = bf16[2,256,2048]{2,1,0:T(8,128)(2,1)} all-to-all(bf16[2,256,2048]{2,1,0:T(8,128)(2,1)S(1)} %broadcast_in_dim.9), channel_id=1, replica_groups=mesh['rep'=2,'fs'=32,'tp'=2] {'tp'}, dimensions={0} | all-to-all | bytes 4194304 | tf_op jit(solution)/shard_map/all_to_all | solution.py:12
  240.7 1.1 broadcast_in_dim.10
  241.8 7.2 %all-to-all-start.3 = ((bf16[32,256,64]{1,2,0:T(8,128)(2,1)}), bf16[32,256,64]{1,2,0:T(8,128)(2,1)}, u32[]{:S(2)}, u32[]{:S(2)}) async-start(bf16[32,256,64]{1,2,0:T(8,128)(2,1)} %broadcast_in_dim.10), calls=%async_computation.3 | async-start | bytes 2097152 | tf_op jit(solution)/shard_map/all_to_all | solution.py:12
  249.0 91.1 %all-gather.9.cloned.1.call-done = bf16[2048,512]{1,0:T(8,128)(2,1)} async-done(((bf16[64,512]{1,0:T(8,128)(2,1)}), bf16[2048,512]{1,0:T(8,128)(2,1)}) %all-gather.9.cloned.1.call-update) | async-done | bytes 2097168 | tf_op jit(solution)/shard_map/all_gather | solution.py:52
  340.2 2.7 fusion.47
  343.3 0.7 convolution_multiply_fusion
  344.0 2.9 fusion.91
  346.9 25.6 %all-gather.2 = f32[2,1,512]{2,1,0:T(1,128)S(1)} all-gather(f32[1,1,512]{2,1,0:T(1,128)S(1)} %bitcast.90), channel_id=2, replica_groups=mesh['rep'=2,'fs'=32,'tp'=2] {'tp'}, dimensions={0}, use_global_device_ids=true | all-gather | bytes 6144 | tf_op jit(solution)/shard_map/all_gather | solution.py:57
  372.6 1.3 multiply_reduce_fusion.2
  373.8 1.8 all-gather.3
  375.7 2.2 convolution_convert_fusion
  377.9 5.4 %all_to_all.37 = bf16[2,256,2048]{2,1,0:T(8,128)(2,1)S(1)} all-to-all(bf16[2,256,2048]{2,1,0:T(8,128)(2,1)S(1)} %bitcast.84), channel_id=1, replica_groups=mesh['rep'=2,'fs'=32,'tp'=2] {'tp'}, dimensions={0} | all-to-all | bytes 4194304 | tf_op jit(solution)/shard_map/all_to_all | solution.py:34
  383.7 0.5 multiply_reduce_fusion
  384.3 0.8 copy-done.1
  385.1 0.6 multiply_convert_fusion
  386.0 5.4 %all_to_all.38 = bf16[2,256,2048]{2,1,0:T(8,128)(2,1)S(1)} all-to-all(bf16[2,256,2048]{2,1,0:T(8,128)(2,1)S(1)} %broadcast_in_dim.11), channel_id=1, replica_groups=mesh['rep'=2,'fs'=32,'tp'=2] {'tp'}, dimensions={0} | all-to-all | bytes 4194304 | tf_op jit(solution)/shard_map/all_to_all | solution.py:12
  391.5 1.4 copy-done.4
  392.8 7.6 %fusion.8 = f32[512,1408]{1,0:T(8,128)} fusion(bf16[512,2048]{1,0:T(8,128)(2,1)S(1)} %bitcast.85, bf16[2048,4224]{1,0:T(8,128)(2,1)} %all-gather.7.cloned.1.call-done), kind=kOutput, calls=%fused_computation.8 | convolution fusion | flops 2952790016 | bytes 10747904 | tf_op jit(solution)/shard_map/dot_general | solution.py:83
  400.4 13.9 %fusion.27 = bf16[512,2048]{1,0:T(8,128)(2,1)} fusion(bf16[2048,4224]{1,0:T(8,128)(2,1)} %all-gather.7.cloned.1.call-done, bf16[512,2048]{1,0:T(8,128)(2,1)} %bitcast.86, f32[512,1408]{1,0:T(8,128)} %fusion.8), kind=kOutput, calls=%fused_computation.21 | convolution fusion | flops 5910953984 | bytes 18612224 | tf_op jit(solution)/shard_map/dot_general | solution.py:135
  414.3 6.6 %all_to_all.39 = bf16[2,256,2048]{2,1,0:T(8,128)(2,1)S(1)} all-to-all(bf16[2,256,2048]{2,1,0:T(8,128)(2,1)} %bitcast.87), channel_id=1, replica_groups=mesh['rep'=2,'fs'=32,'tp'=2] {'tp'}, dimensions={0} | all-to-all | bytes 4194304 | tf_op jit(solution)/shard_map/all_to_all | solution.py:34
  421.4 1.1 copy-done.2
  422.5 1.7 fusion.38
  (49 shorter events, 4.1 us)
Async XLA Ops:
  6.5 2.7 copy-start
  6.5 197.9 %all-gather.7.cloned.1.call-start = ((), (), s32[]{:S(2)}) async-start(), calls=%async_computation.7 | async-start | bytes 17842176 | tf_op jit(solution)/shard_map/all_gather | solution.py:41
  11.5 4.6 %copy-start.7 = (bf16[64,256]{1,0:T(8,128)(2,1)S(1)}, bf16[64,256]{1,0:T(8,128)(2,1)}, u32[]{:S(2)}) copy-start(bf16[64,256]{1,0:T(8,128)(2,1)} %param.20) | copy-start | bytes 98308
  11.5 4.6 %copy-start.8 = (bf16[64,256]{1,0:T(8,128)(2,1)S(1)}, bf16[64,256]{1,0:T(8,128)(2,1)}, u32[]{:S(2)}) copy-start(bf16[64,256]{1,0:T(8,128)(2,1)} %param.19) | copy-start | bytes 98308
  11.5 5.3 %copy-start.5 = (bf16[31,256]{1,0:T(8,128)(2,1)S(1)}, bf16[31,256]{1,0:T(8,128)(2,1)}, u32[]{:S(2)}) copy-start(bf16[31,256]{1,0:T(8,128)(2,1)} %param.21) | copy-start | bytes 47620
  11.5 5.4 %copy-start.12 = (bf16[256]{0:T(256)(128)(2,1)S(1)}, bf16[256]{0:T(256)(128)(2,1)}, u32[]{:S(2)}) copy-start(bf16[256]{0:T(256)(128)(2,1)} %param.22) | copy-start | bytes 1540
  11.5 5.4 %copy-start.9 = (bf16[2048]{0:T(1024)(128)(2,1)S(1)}, bf16[2048]{0:T(1024)(128)(2,1)}, u32[]{:S(2)}) copy-start(bf16[2048]{0:T(1024)(128)(2,1)} %param.14) | copy-start | bytes 12292
  11.5 5.4 %copy-start.10 = (bf16[2048]{0:T(1024)(128)(2,1)S(1)}, bf16[2048]{0:T(1024)(128)(2,1)}, u32[]{:S(2)}) copy-start(bf16[2048]{0:T(1024)(128)(2,1)} %param.15) | copy-start | bytes 12292
  11.5 7.1 %all-to-all-start = ((bf16[2,256,2048]{2,1,0:T(8,128)(2,1)}), bf16[2,256,2048]{2,1,0:T(8,128)(2,1)S(1)}, u32[]{:S(2)}, u32[]{:S(2)}) async-start(bf16[2,256,2048]{2,1,0:T(8,128)(2,1)} %broadcast_in_dim.8), calls=%async_computation | async-start | bytes 4194304 | tf_op jit(solution)/shard_map/all_to_all | solution.py:12
  16.1 324.1 %all-gather.9.cloned.1.call-start = ((), (), s32[]{:S(2)}) async-start(), calls=%async_computation.8 | async-start | bytes 2162688 | tf_op jit(solution)/shard_map/all_gather | solution.py:52
  234.4 6.3 %copy-start.6 = (bf16[256,64]{0,1:T(8,128)(2,1)S(1)}, bf16[256,64]{0,1:T(8,128)(2,1)}, u32[]{:S(2)}) copy-start(bf16[256,64]{0,1:T(8,128)(2,1)} %param.23) | copy-start | bytes 98308
  241.8 133.9 %all-to-all-start.3 = ((bf16[32,256,64]{1,2,0:T(8,128)(2,1)}), bf16[32,256,64]{1,2,0:T(8,128)(2,1)}, u32[]{:S(2)}, u32[]{:S(2)}) async-start(bf16[32,256,64]{1,2,0:T(8,128)(2,1)} %broadcast_in_dim.10), calls=%async_computation.3 | async-start | bytes 2097152 | tf_op jit(solution)/shard_map/all_to_all | solution.py:12
  340.2 2.7 copy-start.3
  340.2 3.2 copy-start.11
  383.7 1.4 copy-start.1
  391.5 1.4 copy-start.4
  420.9 1.6 copy-start.2
Sparse Core Ops, SparseCore 0:
  9.0 195.4 all-gather.6
  206.1 133.9 all-gather.8
where the time goes:
time: 432 us; the launch traced here: 431 us
  waiting for transfers between devices  279 us (65%)
  blocking collectives  58.6 us (14%)
  matrix products  48 us (11%)
  between operations  13.6 us (3%)
  other arithmetic  13.3 us (3%)
  starting transfers between devices  11.7 us (3%)
  local copies, waits for them, and re-layouts  7 us (2%)
    all_gather x1, waiting for transfers between devices, rows_first(): lax.all_gather(both, axis, axis=0, tiled=True)  186 us
    all_gather x1, waiting for transfers between devices, in_one_piece(): filled = lax.all_gather(both, axis, axis=dim, tiled=True)  91.1 us
    all_gather x2, blocking collectives, over_pieces(): return lax.all_gather(x, axis).sum(0)  27.4 us
    all_to_all x3, blocking collectives, sent_and_summed(): pieces = lax.all_to_all(split_up(x, dim, count), axis, 0, 0, tiled=True)  19.5 us
    dot_general x2, matrix products, hidden_units(): jnp.dot(gathered, whole_gate, preferred_element_type=jnp.float32)  15.2 us
    dot_general x1, matrix products, shards(): jnp.dot(second_hidden, whole_down, preferred_element_type=jnp.float32)  13.9 us
    dot_general x1, matrix products, shards(): first_out = jnp.dot(hidden, whole_down, preferred_element_type=jnp.float32)  13.3 us
    all_to_all x2, starting transfers between devices, sent_to_all(): return lax.all_to_all(copies, axis, split_axis=0, concat_axis=0, tiled=True)  11.7 us
  transfers between devices with their start and end apart: 4, of which 3 were waited for; matrix products, arithmetic and copies ran while one was open for 8% of the time, Pallas kernels for 0%

commit v1 on v0

v1 whole, which is shorter than its diff:
```python
import jax
import jax.numpy as jnp
from jax import lax
from jax.sharding import PartitionSpec as P

ROW_EPS = 0.05
CHAN_EPS = 0.02
SWAP = [(0, 1), (1, 0)]


def other(x):
    return lax.ppermute(x, "tp", SWAP)


def rms_rows(stream, gain_vec):
    square_mean = jnp.mean(stream * stream, axis=-1, keepdims=True)
    return (stream * lax.rsqrt(square_mean + ROW_EPS) * gain_vec.astype(jnp.float32)).astype(
        jnp.bfloat16
    )


def dot(a, b):
    return jnp.dot(a, b, preferred_element_type=jnp.float32)


def dot_t(a, b):
    return lax.dot_general(a, b, (((1,), (1,)), ((), ())), preferred_element_type=jnp.float32)


def feed(normed, gate, up, down_a, down_b):
    cut = down_a.shape[1]
    rows = jnp.concatenate([normed, other(normed)], axis=0)
    hidden = (jax.nn.silu(dot(rows, gate)) * dot(rows, up)).astype(jnp.bfloat16)
    half = normed.shape[0]

    def down(part):
        return dot_t(part[:, :cut], down_a) + dot_t(part[:, cut:], down_b)

    theirs = down(hidden[half:]).astype(jnp.bfloat16)
    received = other(theirs)
    return down(hidden[:half]) + received.astype(jnp.float32)


def causal_taps(padded, kernel, length):
    output = jnp.zeros((length, padded.shape[1]), jnp.float32)
    for tap_index in range(kernel.shape[0]):
        output = output + padded[tap_index : tap_index + length] * kernel[tap_index]
    return output


def shards(
    tokens,
    norm_first,
    norm_mixer,
    norm_second,
    ffn_gate,
    ffn_up,
    ffn_down,
    conv_value,
    conv_gate,
    depthwise,
    conv_gain,
    conv_out,
):
    width = tokens.shape[-1]
    tp = lax.axis_index("tp")
    rep = lax.axis_index("rep")
    n = ffn_gate.shape[1]
    c = conv_value.shape[1]
    down_t = ffn_down.T
    out_t = conv_out.T
    total = 20 * 128
    a_down = total - n - 2 * c
    b_down = total - n - c
    part0 = jnp.concatenate([ffn_gate, conv_value, conv_gate, down_t[:, :a_down]], axis=1)
    part1 = jnp.concatenate([ffn_up, out_t, down_t[:, n - b_down :]], axis=1)
    mine = jnp.where(rep == 0, part0, part1)
    full = lax.all_gather(mine, ("rep", "fs"), axis=0, tiled=True)
    first, second = full[:width], full[width:]
    gate, up = first[:, :n], second[:, :n]
    down_a = first[:, n + 2 * c :]
    down_b = second[:, n + c + (a_down + b_down - n) :]
    value_gate = first[:, n : n + 2 * c]
    out_half = second[:, n : n + c]
    value_gate_o = other(value_gate)
    out_half_o = other(out_half)
    taps = jnp.concatenate([depthwise, conv_gain[None, :]], axis=0).astype(jnp.float32)
    taps_o = other(taps)

    stream = tokens.reshape(-1, width).astype(jnp.float32)
    length = stream.shape[0]
    stream = stream + 0.5 * feed(rms_rows(stream, norm_first), gate, up, down_a, down_b)

    normed = rms_rows(stream, norm_mixer)
    both, both_o = dot(normed, value_gate), dot(normed, value_gate_o)
    glu = jnp.concatenate(
        [both[:, :c] * jax.nn.sigmoid(both[:, c:]), both_o[:, :c] * jax.nn.sigmoid(both_o[:, c:])],
        axis=1,
    )
    kernel = jnp.concatenate([taps, taps_o], axis=1)
    reach = depthwise.shape[0] - 1
    tail = glu[length - reach :]
    swapped = jnp.concatenate([tail[:, c:], tail[:, :c]], axis=1)
    before = jnp.where(tp == 1, other(swapped), 0.0)
    conv = causal_taps(jnp.concatenate([before, glu], axis=0), kernel[:-1], length)
    average = jnp.mean(conv, axis=1, keepdims=True)
    centred = conv - average
    spread = jnp.mean(centred * centred, axis=1, keepdims=True)
    activated = jax.nn.silu(centred * lax.rsqrt(spread + CHAN_EPS) * kernel[-1]).astype(jnp.bfloat16)
    stream = stream + dot_t(activated[:, :c], out_half) + dot_t(activated[:, c:], out_half_o)

    stream = stream + 0.5 * feed(rms_rows(stream, norm_second), gate, up, down_a, down_b)
    return stream.astype(jnp.bfloat16).reshape(tokens.shape)


def solution(mesh):
    in_specs = (
        P(("rep", "fs"), "tp", None),
        P(),
        P(),
        P(),
        P("fs", "tp"),
        P("fs", "tp"),
        P("tp", "fs"),
        P("fs", "tp"),
        P("fs", "tp"),
        P(None, "tp"),
        P("tp"),
        P("tp", "fs"),
    )
    out_specs = P(("rep", "fs"), "tp", None)
    return jax.shard_map(shards, mesh=mesh, in_specs=in_specs, out_specs=out_specs, check_vma=False)
```

time: 432 us -> 199 us (0.46)
  waiting for transfers between devices: 279 us -> 125 us
  blocking collectives: 58.6 us -> 0 us
  starting transfers between devices: 11.7 us -> 3.58 us
  other arithmetic: 13.3 us -> 6.84 us
    all_gather x2 -> x1, waiting for transfers between devices: 277 us -> 115 us  [shards(): full = lax.all_gather(mine, ('rep', 'fs'), axis=0, tiled=True)]
    all_to_all x5 -> x0, blocking collectives: 31.2 us -> none  [the longest x3 19.5 us: sent_and_summed(): pieces = lax.all_to_all(split_up(x, dim, count), axis, 0, 0, tiled=True)]
    all_gather x2 -> x0, blocking collectives: 27.4 us -> none  [over_pieces(): return lax.all_gather(x, axis).sum(0)]
    all_to_all x2 -> x0, starting transfers between devices: 11.7 us -> none  [sent_to_all(): return lax.all_to_all(copies, axis, split_axis=0, concat_axis=0, tiled=True)]
    ppermute x0 -> x8, waiting for transfers between devices: none -> 9.96 us  [other(): return lax.ppermute(x, 'tp', SWAP)]
    slice x2 -> x6, local copies, waits for them, and re-layouts: 0.03 us -> 4.95 us  [the longest x1 1.75 us: shards(): value_gate = first[:, n:n + 2 * c]]
    dot_general x7 -> x16, matrix products: 48 us -> 43.7 us  [the longest x6 23.6 us: dot(): return jnp.dot(a, b, preferred_element_type=jnp.float32)]
  transfers between devices with their start and end apart: 4 -> 9, of which waited for: 3 -> 5; matrix products, arithmetic and copies ran while one was open for 8% -> 9% of each run, Pallas kernels for 0% -> 0%
where the time goes in v1:
time: 199 us; the launch traced here: 198 us
  waiting for transfers between devices  125 us (63%)
  matrix products  43.7 us (22%)
  between operations  13.8 us (7%)
  other arithmetic  6.84 us (3%)
  local copies, waits for them, and re-layouts  5 us (3%)
  starting transfers between devices  3.58 us (2%)
    all_gather x1, waiting for transfers between devices, shards(): full = lax.all_gather(mine, ('rep', 'fs'), axis=0, tiled=True)  115 us
    dot_general x6, matrix products, dot(): return jnp.dot(a, b, preferred_element_type=jnp.float32)  23.6 us
    dot_general x10, matrix products, dot_t(): lax.dot_general(a, b, (((1,), (1,)), ((), ())), preferred_element_type=jn...  20.1 us
    ppermute x8, waiting for transfers between devices, other(): return lax.ppermute(x, 'tp', SWAP)  9.96 us
  transfers between devices with their start and end apart: 9, of which 5 were waited for; matrix products, arithmetic and copies ran while one was open for 9% of the time, Pallas kernels for 0%

profile of v1, /device:TPU:3, one launch (start us, length us, event | category | flops | bytes accessed | tf_op | source)
XLA Modules:
  0.0 198.1 jit_solution(7628016379162098751)
XLA Ops:
  6.5 1.0 slice.402
  7.5 0.9 slice.401
  8.4 1.9 maximum_select_fusion
  10.3 0.7 convert_element_type.53
  11.6 0.8 collective-permute-start
  12.4 2.3 %collective-permute-done = bf16[256,2048]{1,0:T(8,128)(2,1)S(1)} collective-permute-done((bf16[256,2048]{1,0:T(8,128)(2,1)S(1)}, bf16[256,2048]{1,0:T(8,128)(2,1)S(1)}, u32[]{:S(2)}, u32[]{:S(2)}) %collective-permute-start) | collective-permute-done | bytes 1048608 | tf_op jit(solution)/shard_map/ppermute | solution.py:12
  14.7 115.2 %all-gather.2.cloned.1.call-done = bf16[4096,2560]{1,0:T(8,128)(2,1)} async-done(((bf16[64,2560]{1,0:T(8,128)(2,1)}), bf16[4096,2560]{1,0:T(8,128)(2,1)}) %all-gather.2.cloned.1.call-update) | async-done | bytes 20971536 | tf_op jit(solution)/shard_map/all_gather | solution.py:78
  129.8 5.7 %fusion.6 = f32[512,1408]{1,0:T(8,128)S(1)} fusion(bf16[4096,2560]{1,0:T(8,128)(2,1)} %all-gather.2.cloned.1.call-done, bf16[256,2048]{1,0:T(8,128)(2,1)S(1)} %collective-permute-done, bf16[256,2048]{1,0:T(8,128)(2,1)S(1)} %fusion.13), kind=kOutput, calls=%fused_computation.6 | convolution fusion | flops 2956984320 | bytes 10747904 | tf_op jit(solution)/shard_map/dot_general | solution.py:23
  135.6 6.2 %multiply_convert_fusion.1 = bf16[512,1408]{1,0:T(8,128)(2,1)S(1)} fusion(f32[512,1408]{1,0:T(8,128)S(1)} %fusion.6, bf16[4096,2560]{1,0:T(8,128)(2,1)} %all-gather.2.cloned.1.call-done, bf16[256,2048]{1,0:T(8,128)(2,1)S(1)} %collective-permute-done, bf16[256,2048]{1,0:T(8,128)(2,1)S(1)} %fusion.13), kind=kOutput, calls=%fused_computation.12 | convolution fusion | flops 2961309696 | bytes 12189696 | tf_op jit(solution)/shard_map/dot_general | solution.py:23
  141.7 3.4 %fusion.18 = f32[256,2048]{1,0:T(8,128)S(1)} fusion(bf16[4096,2560]{1,0:T(8,128)(2,1)} %all-gather.2.cloned.1.call-done, bf16[512,1408]{1,0:T(8,128)(2,1)S(1)} %multiply_convert_fusion.1), kind=kOutput, calls=%fused_computation.35 | convolution fusion | flops 805306368 | bytes 5636096 | tf_op jit(solution)/shard_map/dot_general | solution.py:27
  145.2 3.8 %fusion.9 = bf16[256,2048]{1,0:T(8,128)(2,1)} fusion(f32[256,2048]{1,0:T(8,128)S(1)} %fusion.18, bf16[4096,2560]{1,0:T(8,128)(2,1)} %all-gather.2.cloned.1.call-done, bf16[512,1408]{1,0:T(8,128)(2,1)S(1)} %multiply_convert_fusion.1), kind=kOutput, calls=%fused_computation.19 | convolution fusion | flops 672137216 | bytes 6094848 | tf_op jit(solution)/shard_map/dot_general | solution.py:27
  149.0 0.8 collective-permute-start.1
  149.9 1.7 slice.411
  151.7 0.6 collective-permute-start.4
  152.3 3.7 %collective-permute-done.4 = f32[32,256]{1,0:T(8,128)S(1)} collective-permute-done((f32[32,256]{1,0:T(8,128)S(1)}, f32[32,256]{1,0:T(8,128)S(1)}, u32[]{:S(2)}, u32[]{:S(2)}) %collective-permute-start.4) | collective-permute-done | bytes 32800 | tf_op jit(solution)/shard_map/ppermute | solution.py:12
  156.0 3.0 %fusion.20 = f32[256,2048]{1,0:T(8,128)S(1)} fusion(bf16[4096,2560]{1,0:T(8,128)(2,1)} %all-gather.2.cloned.1.call-done, bf16[512,1408]{1,0:T(8,128)(2,1)} %copy-done.1), kind=kOutput, calls=%fused_computation.37 | convolution fusion | flops 805306368 | bytes 5636096 | tf_op jit(solution)/shard_map/dot_general | solution.py:27
  159.1 3.6 %multiply_reduce_fusion.1 = (f32[256]{0:T(256)S(1)}, f32[256,2048]{1,0:T(8,128)S(1)}) fusion(bf16[256,2048]{1,0:T(8,128)(2,1)} %collective-permute-done.1, f32[256,2048]{1,0:T(8,128)S(1)} %fusion.20, bf16[4096,2560]{1,0:T(8,128)(2,1)} %all-gather.2.cloned.1.call-done, bf16[512,1408]{1,0:T(8,128)(2,1)} %copy-done.1, bf16[1,256,2048]{2,1,0:T(8,128)(2,1)S(1)} %copy-done), kind=kOutput, calls=%fused_computation.30 | convolution fusion | flops 675282688 | bytes 9241600 | tf_op jit(solution)/shard_map/dot_general | solution.py:27
  162.7 2.4 %fusion.122 = f32[256,512]{1,0:T(8,128)S(1)} fusion(f32[256,2048]{1,0:T(8,128)S(1)} %get-tuple-element.40, f32[2048]{0:T(1024)S(1)} %convert_element_type.58, f32[256]{0:T(256)S(1)} %add_rsqrt_fusion.2, bf16[4096,2560]{1,0:T(8,128)(2,1)} %all-gather.2.cloned.1.call-done), kind=kOutput, calls=%fused_computation.237 | convolution fusion | flops 538443776 | bytes 4727808 | tf_op jit(solution)/shard_map/dot_general | solution.py:23
  165.2 2.5 %fusion.123 = f32[256,512]{1,0:T(8,128)S(1)} fusion(bf16[2048,512]{1,0:T(8,128)(2,1)} %collective-permute-done.2, f32[256,2048]{1,0:T(8,128)S(1)} %get-tuple-element.40, f32[2048]{0:T(1024)S(1)} %convert_element_type.58, f32[256]{0:T(256)S(1)} %add_rsqrt_fusion.2), kind=kOutput, calls=%fused_computation.238 | convolution fusion | flops 538443776 | bytes 4727808 | tf_op jit(solution)/shard_map/dot_general | solution.py:23
  168.1 1.3 slice.511
  169.4 0.6 collective-permute-start.5
  170.1 2.6 %fusion.125 = (f32[256]{0:T(256)S(1)}, f32[256,512]{1,0:T(8,128)S(1)}) fusion(f32[512]{0:T(512)S(1)} %bitcast.52, f32[256,256]{1,0:T(8,128)S(1)} %fusion.82, f32[256,256]{1,0:T(8,128)S(1)} %fusion.78, f32[512]{0:T(512)S(1)} %bitcast.51, f32[286,512]{1,0:T(8,128)S(1)} %maximum_maximum_fusion, f32[512]{0:T(512)S(1)} %bitcast.50, f32[512]{0:T(512)S(1)} %bitcast.49, ...), kind=kLoop, calls=%fused_computation.240 | loop fusion | flops 8257280 | bytes 16841728 | tf_op jit(solution)/shard_map/reduce_sum | solution.py:106
  173.2 0.5 fusion.83
  173.8 0.6 multiply_reduce_fusion
  174.9 2.5 %collective-permute-done.6 = bf16[256,2048]{1,0:T(8,128)(2,1)S(1)} collective-permute-done((bf16[256,2048]{1,0:T(8,128)(2,1)S(1)}, bf16[256,2048]{1,0:T(8,128)(2,1)S(1)}, u32[]{:S(2)}, u32[]{:S(2)}) %collective-permute-start.6) | collective-permute-done | bytes 1048608 | tf_op jit(solution)/shard_map/ppermute | solution.py:12
  177.4 3.4 %fusion.4 = f32[512,1408]{1,0:T(8,128)S(1)} fusion(bf16[4096,2560]{1,0:T(8,128)(2,1)S(1)} %bitcast.44, bf16[256,2048]{1,0:T(8,128)(2,1)S(1)} %collective-permute-done.6, bf16[256,2048]{1,0:T(8,128)(2,1)S(1)} %multiply_convert_fusion.2), kind=kOutput, calls=%fused_computation.4 | convolution fusion | flops 2956984320 | bytes 10747904 | tf_op jit(solution)/shard_map/dot_general | solution.py:23
  180.8 3.5 %multiply_convert_fusion = bf16[512,1408]{1,0:T(8,128)(2,1)S(1)} fusion(f32[512,1408]{1,0:T(8,128)S(1)} %fusion.4, bf16[4096,2560]{1,0:T(8,128)(2,1)S(1)} %bitcast.44, bf16[256,2048]{1,0:T(8,128)(2,1)S(1)} %collective-permute-done.6, bf16[256,2048]{1,0:T(8,128)(2,1)S(1)} %multiply_convert_fusion.2), kind=kOutput, calls=%fused_computation.11 | convolution fusion | flops 2961309696 | bytes 12189696 | tf_op jit(solution)/shard_map/dot_general | solution.py:23
  184.3 1.0 fusion.14
  185.3 1.1 fusion.10
  186.6 1.0 fusion.16
  187.6 1.5 collective-permute-done.7
  189.1 2.1 %fusion.30 = bf16[1,256,2048]{2,1,0:T(8,128)(2,1)} fusion(f32[256,2048]{1,0:T(8,128)S(1)} %get-tuple-element.42, bf16[256,2048]{1,0:T(8,128)(2,1)S(1)} %collective-permute-done.7, f32[256,2048]{1,0:T(8,128)S(1)} %fusion.16, bf16[4096,2560]{1,0:T(8,128)(2,1)S(1)} %bitcast.44, bf16[512,1408]{1,0:T(8,128)(2,1)S(1)} %multiply_convert_fusion), kind=kOutput, calls=%fused_computation.43 | convolution fusion | flops 674234368 | bytes 9240576 | tf_op jit(solution)/shard_map/dot_general | solution.py:27
  (58 shorter events, 2.6 us)
Async XLA Ops:
  6.5 4.5 %copy-start = (bf16[1,256,2048]{2,1,0:T(8,128)(2,1)S(1)}, bf16[1,256,2048]{2,1,0:T(8,128)(2,1)}, u32[]{:S(2)}) copy-start(bf16[1,256,2048]{2,1,0:T(8,128)(2,1)} %param.12) | copy-start | bytes 3145732
  6.5 123.3 %all-gather.2.cloned.1.call-start = ((), (), s32[]{:S(2)}) async-start(), calls=%async_computation | async-start | bytes 21299200 | tf_op jit(solution)/shard_map/all_gather | solution.py:78
  11.6 3.0 %collective-permute-start = (bf16[256,2048]{1,0:T(8,128)(2,1)S(1)}, bf16[256,2048]{1,0:T(8,128)(2,1)S(1)}, u32[]{:S(2)}, u32[]{:S(2)}) collective-permute-start(bf16[256,2048]{1,0:T(8,128)(2,1)S(1)} %fusion.13), channel_id=1, source_target_pairs={{0,1},{1,0},{2,3},{3,2},{4,5},{5,4},{6,7},{7,6},{8,9},{9,8},{10,11... | collective-permute-start | bytes 3145736 | tf_op jit(solution)/shard_map/ppermute | solution.py:12
  141.7 3.5 %copy-start.1 = (bf16[512,1408]{1,0:T(8,128)(2,1)}, bf16[512,1408]{1,0:T(8,128)(2,1)S(1)}, u32[]{:S(2)}) copy-start(bf16[512,1408]{1,0:T(8,128)(2,1)S(1)} %multiply_convert_fusion.1) | copy-start | bytes 4325380
  145.2 4.6 %copy-start.5 = (bf16[256]{0:T(256)(128)(2,1)S(1)}, bf16[256]{0:T(256)(128)(2,1)}, u32[]{:S(2)}) copy-start(bf16[256]{0:T(256)(128)(2,1)} %param.22) | copy-start | bytes 1540
  149.0 10.1 %collective-permute-start.1 = (bf16[256,2048]{1,0:T(8,128)(2,1)}, bf16[256,2048]{1,0:T(8,128)(2,1)}, u32[]{:S(2)}, u32[]{:S(2)}) collective-permute-start(bf16[256,2048]{1,0:T(8,128)(2,1)} %fusion.9), channel_id=1, source_target_pairs={{0,1},{1,0},{2,3},{3,2},{4,5},{5,4},{6,7},{7,6},{8,9},{9,8},{10,11... | collective-permute-start | bytes 3145736 | tf_op jit(solution)/shard_map/ppermute | solution.py:12
  149.8 1.9 copy-start.2
  149.8 2.5 %copy-start.3 = (bf16[2048]{0:T(1024)(128)(2,1)S(1)}, bf16[2048]{0:T(1024)(128)(2,1)}, u32[]{:S(2)}) copy-start(bf16[2048]{0:T(1024)(128)(2,1)} %param.14) | copy-start | bytes 12292
  149.8 2.5 %copy-start.4 = (bf16[2048]{0:T(1024)(128)(2,1)S(1)}, bf16[2048]{0:T(1024)(128)(2,1)}, u32[]{:S(2)}) copy-start(bf16[2048]{0:T(1024)(128)(2,1)} %param.15) | copy-start | bytes 12292
  151.6 13.6 %collective-permute-start.2 = (bf16[2048,512]{1,0:T(8,128)(2,1)S(1)}, bf16[2048,512]{1,0:T(8,128)(2,1)}, u32[]{:S(2)}, u32[]{:S(2)}) collective-permute-start(bf16[2048,512]{1,0:T(8,128)(2,1)S(1)} %slice.411), channel_id=1, source_target_pairs={{0,1},{1,0},{2,3},{3,2},{4,5},{5,4},{6,7},{7,6},{8,9},{9,8},{10,11... | collective-permute-start | bytes 6291464 | tf_op jit(solution)/shard_map/ppermute | solution.py:12
  151.7 4.3 %collective-permute-start.4 = (f32[32,256]{1,0:T(8,128)S(1)}, f32[32,256]{1,0:T(8,128)S(1)}, u32[]{:S(2)}, u32[]{:S(2)}) collective-permute-start(f32[32,256]{1,0:T(8,128)S(1)} %maximum_convert_fusion), channel_id=1, source_target_pairs={{0,1},{1,0},{2,3},{3,2},{4,5},{5,4},{6,7},{7,6},{8,9},{9,8},{10,11... | collective-permute-start | bytes 98312 | tf_op jit(solution)/shard_map/ppermute | solution.py:12
  159.1 14.6 %slice-start = ((s8[20971520]{0:T(1024)(128)(4,1)}), s8[4194304]{0:T(1024)(128)(4,1)S(1)}, s32[]{:S(2)}) async-start(s8[20971520]{0:T(1024)(128)(4,1)} %bitcast.43), calls=%async_computation.1 | async-start | bytes 8388608
  159.1 14.6 %slice-start.1 = ((s8[20971520]{0:T(1024)(128)(4,1)}), s8[4194304]{0:T(1024)(128)(4,1)S(1)}, s32[]{:S(2)}) async-start(s8[20971520]{0:T(1024)(128)(4,1)} %bitcast.43), calls=%async_computation.2 | async-start | bytes 8388608
  165.2 8.5 %slice-start.2 = ((s8[20971520]{0:T(1024)(128)(4,1)}), s8[4194304]{0:T(1024)(128)(4,1)S(1)}, s32[]{:S(2)}) async-start(s8[20971520]{0:T(1024)(128)(4,1)} %bitcast.43), calls=%async_computation.3 | async-start | bytes 8388608
  167.8 2.2 %collective-permute-start.3 = (f32[30,512]{1,0:T(8,128)S(1)}, f32[30,512]{1,0:T(8,128)S(1)}, u32[]{:S(2)}, u32[]{:S(2)}) collective-permute-start(f32[30,512]{1,0:T(8,128)S(1)} %pad_maximum_fusion.10), channel_id=1, source_target_pairs={{0,1},{1,0},{2,3},{3,2},{4,5},{5,4},{6,7},{7,6},{8,9},{9,8},{10,11... | collective-permute-start | bytes 184328 | tf_op jit(solution)/shard_map/ppermute | solution.py:12
  169.4 3.8 %collective-permute-start.5 = (bf16[2048,256]{1,0:T(8,128)(2,1)S(1)}, bf16[2048,256]{1,0:T(8,128)(2,1)S(1)}, u32[]{:S(2)}, u32[]{:S(2)}) collective-permute-start(bf16[2048,256]{1,0:T(8,128)(2,1)S(1)} %slice.511), channel_id=1, source_target_pairs={{0,1},{1,0},{2,3},{3,2},{4,5},{5,4},{6,7},{7,6},{8,9},{9,8},{10,11... | collective-permute-start | bytes 3145736 | tf_op jit(solution)/shard_map/ppermute | solution.py:12
  170.1 3.7 %slice-start.3 = ((s8[20971520]{0:T(1024)(128)(4,1)}), s8[4194304]{0:T(1024)(128)(4,1)S(1)}, s32[]{:S(2)}) async-start(s8[20971520]{0:T(1024)(128)(4,1)} %bitcast.43), calls=%async_computation.4 | async-start | bytes 8388608
  170.1 3.7 %slice-start.4 = ((s8[20971520]{0:T(1024)(128)(4,1)}), s8[4194304]{0:T(1024)(128)(4,1)S(1)}, s32[]{:S(2)}) async-start(s8[20971520]{0:T(1024)(128)(4,1)} %bitcast.43), calls=%async_computation.5 | async-start | bytes 8388608
  174.6 2.7 %collective-permute-start.6 = (bf16[256,2048]{1,0:T(8,128)(2,1)S(1)}, bf16[256,2048]{1,0:T(8,128)(2,1)S(1)}, u32[]{:S(2)}, u32[]{:S(2)}) collective-permute-start(bf16[256,2048]{1,0:T(8,128)(2,1)S(1)} %multiply_convert_fusion.2), channel_id=1, source_target_pairs={{0,1},{1,0},{2,3},{3,2},{4,5},{5,4},{6,7},{7,6},{8,9},{9,8},{10,11... | collective-permute-start | bytes 3145736 | tf_op jit(solution)/shard_map/ppermute | solution.py:12
  186.3 2.7 %collective-permute-start.7 = (bf16[256,2048]{1,0:T(8,128)(2,1)S(1)}, bf16[256,2048]{1,0:T(8,128)(2,1)S(1)}, u32[]{:S(2)}, u32[]{:S(2)}) collective-permute-start(bf16[256,2048]{1,0:T(8,128)(2,1)S(1)} %fusion.10), channel_id=1, source_target_pairs={{0,1},{1,0},{2,3},{3,2},{4,5},{5,4},{6,7},{7,6},{8,9},{9,8},{10,11... | collective-permute-start | bytes 3145736 | tf_op jit(solution)/shard_map/ppermute | solution.py:12
Sparse Core Ops, SparseCore 0:
  10.4 119.3 all-gather.1

commit v2 on v1

v2 whole, which is shorter than its diff:
```python
import jax
import jax.numpy as jnp
from jax import lax
from jax.experimental import pallas as pl
from jax.experimental.pallas import tpu as pltpu
from jax.sharding import Mesh
from jax.sharding import PartitionSpec as P

ROW_EPS = 0.05
CHAN_EPS = 0.02
SWAP = [(0, 1), (1, 0)]
ALL = ("zh", "zl", "y", "x", "tp")
WIDE = (("x", "y", "z"), ("y", "z", "x"))
NARROW = ("z", "x", "y")
FIRST_WIDE, FIRST_NARROW = 896, 512
ANY = pl.BlockSpec(memory_space=pl.ANY)
SMEM = pl.BlockSpec(memory_space=pltpu.SMEM)


def other(x):
    return lax.ppermute(x, "tp", SWAP)


def from_ring(x, dims, offsets):
    pairs = []
    for z in range(4):
        for y in range(4):
            for x_ in range(4):
                for tp in range(2):
                    source = {"z": z, "y": y, "x": x_}
                    source[dims[tp]] = (source[dims[tp]] + offsets[tp]) % 4
                    at = ((source["z"] * 4 + source["y"]) * 4 + source["x"]) * 2 + tp
                    pairs.append((at, ((z * 4 + y) * 4 + x_) * 2 + tp))
    return lax.ppermute(x, ALL, pairs)


def copied(coords, pieces, outs, plan):
    count = len(pieces)

    def body(coords_ref, *refs):
        sems = refs[-1]
        where = {d: coords_ref[i] for i, d in enumerate(("x", "y", "z", "tp"))}
        made = refs[count:-1]
        for place, length, copies in plan(where, refs[:count]):

            def step(i, carry=0, copies=copies):
                for source, out, index in copies(i):
                    pltpu.make_async_copy(source, made[out].at[index], sems.at[out]).start()
                return carry

            def run(length=length, step=step):
                lax.fori_loop(0, length, step, 0) if length > 1 else step(0)

            if place is None:
                run()
            else:
                pl.when(where["tp"] == place)(run)
        for out, ref in enumerate(made):
            pltpu.make_async_copy(ref, ref, sems.at[out]).wait()

    return pl.pallas_call(
        body,
        in_specs=[SMEM] + [ANY] * count,
        out_specs=[ANY] * len(outs),
        out_shape=[pltpu.VMEM(s, jnp.bfloat16) for s in outs],
        scratch_shapes=[pltpu.SemaphoreType.DMA((len(outs),))],
        compiler_params=pltpu.CompilerParams(vmem_limit_bytes=1 << 20),
    )(coords, *pieces)


def packed(coords, gate, up, down_t, value, gates, out_t):
    rows = gate.shape[0]

    def plan(where, ins):
        half = pl.ds(pl.multiple_of(where["z"] // 2 * (rows // 2), rows // 2), rows // 2)
        every = slice(None)
        copies, at = [], 0
        for ref, width in zip(ins, (FIRST_WIDE, FIRST_WIDE, 768, 256, 256, 256)):
            copies.append((ref.at[half, pl.ds(0, width)], 0, (every, pl.ds(at, width))))
            at += width
        at = 0
        for ref, start in zip(ins, (FIRST_WIDE, FIRST_WIDE, 768)):
            width = ref.shape[1] - start
            copies.append((ref.at[:, pl.ds(start, width)], 1, (every, pl.ds(at, width))))
            at += width
        return [(None, 1, lambda i: copies)]

    outs = [(rows // 2, 3328), (rows, 1664)]
    arrays = (gate, up, down_t, value, gates, out_t)
    arrays = [pltpu.with_memory_space_constraint(x, pltpu.HBM) for x in arrays]
    return copied(coords, arrays, outs, plan)


def wide_at(where, phase):
    return jnp.where(where["tp"] == 0, where[WIDE[0][phase]], where[WIDE[1][phase]])


def in_order(at, pieces, first_out, cuts):
    for k, piece in enumerate(pieces):
        for out, (start, stop) in enumerate(zip(cuts, cuts[1:])):
            source = piece.at[..., pl.ds(start, stop - start)]
            yield source, first_out + out, (at + k) % len(pieces)


def ring_of(x, dims):
    return [x] + [from_ring(x, dims, (k, k)) for k in (1, 2, 3)]


def ring_passed_on(x, dims, ways):
    near = from_ring(x, dims, ways)
    far = from_ring(near, dims, ways)
    last = from_ring(x, dims, tuple((-w) % 4 for w in ways))
    return [x, near, far, last]


def by_way(pieces, way):
    return list(pieces) if way == 1 else [pieces[0], pieces[3], pieces[2], pieces[1]]


def in_rows(coords, wides, narrows, wide_way, narrow_ways, cuts):
    every, parts = slice(None), len(cuts) - 1

    def plan(where, ins):
        def cut(piece, at):
            for part, start, stop in zip(range(parts), cuts, cuts[1:]):
                yield piece.at[..., pl.ds(start, stop - start)], part, at

        def by_z(_):
            for k, piece in enumerate(by_way(ins[:4], wide_way)):
                z = (where["z"] + k) % 4
                yield from cut(piece, (z % 2, every, every, z // 2))

        def by_x(z):
            for k, piece in enumerate(by_way(ins[:4], wide_way)):
                yield from cut(piece.at[z], (z % 2, every, (where["x"] + k) % 4, z // 2))

        def by_y(way):
            def of(zl):
                for k, piece in enumerate(by_way(ins[4:], way)):
                    yield piece.at[:, zl], parts, (zl, (where["y"] + k) % 4)

            return of

        return [
            (0, 1, by_z),
            (1, 4, by_x),
            (0, 2, by_y(narrow_ways[0])),
            (1, 2, by_y(narrow_ways[1])),
        ]

    outs = [(2, 4, 4, 2, 32, b - a) for a, b in zip(cuts, cuts[1:])]
    outs.append((2, 4, 4, 64, narrows[0].shape[-1]))
    return [x.reshape(-1, x.shape[-1]) for x in copied(coords, (*wides, *narrows), outs, plan)]


def gathered(coords, wide, narrow):
    def dims(phase):
        return (WIDE[0][phase], WIDE[1][phase])

    def same(phase):
        return (NARROW[phase],) * 2

    hold = lax.optimization_barrier
    pieces = hold((*ring_of(wide, dims(0)), narrow, from_ring(narrow, same(0), (1, 3))))
    wide, narrow = hold(
        tuple(
            copied(
                coords,
                pieces,
                [(4, *wide.shape), (2, *narrow.shape)],
                lambda where, ins: [
                    (None, 1, lambda i: in_order(wide_at(where, 0), ins[:4], 0, (0, wide.shape[-1]))),
                    (None, 1, lambda i: in_order(where["z"] % 2, ins[4:], 1, (0, narrow.shape[-1]))),
                ],
            )
        )
    )
    pieces = hold((*ring_of(wide, dims(1)), *ring_of(narrow, same(1))))
    cut_wide, cut_narrow = 2 * FIRST_WIDE, 2 * FIRST_NARROW
    shapes = [
        (4, *wide.shape[:-1], cut_wide),
        (4, *wide.shape[:-1], wide.shape[-1] - cut_wide),
        (4, *narrow.shape[:-1], cut_narrow),
        (4, *narrow.shape[:-1], narrow.shape[-1] - cut_narrow),
    ]
    w0, w1, n0, n1 = hold(
        tuple(
            copied(
                coords,
                pieces,
                shapes,
                lambda where, ins: [
                    (None, 1, lambda i: in_order(wide_at(where, 1), ins[:4], 0, (0, cut_wide, wide.shape[-1]))),
                    (None, 1, lambda i: in_order(where["x"], ins[4:], 2, (0, cut_narrow, narrow.shape[-1]))),
                ],
            )
        )
    )
    w0 = ring_passed_on(w0, dims(2), (1, 1))
    w1 = ring_passed_on(w1, dims(2), (3, 3))
    n0 = ring_passed_on(n0, same(2), (1, 3))
    n1 = ring_passed_on(n1, same(2), (3, 1))
    first = in_rows(coords, w0, n0, 1, (1, 3), (0, cut_wide))
    second = in_rows(coords, w1, n1, 3, (3, 1), (0, 768, 1280, 1536))
    return first, second


def rms_rows(stream, gain_vec):
    square_mean = jnp.mean(stream * stream, axis=-1, keepdims=True)
    return (stream * lax.rsqrt(square_mean + ROW_EPS) * gain_vec.astype(jnp.float32)).astype(
        jnp.bfloat16
    )


def dot(a, b):
    return jnp.dot(a, b, preferred_element_type=jnp.float32)


def dot_t(a, b):
    return lax.dot_general(a, b, (((1,), (1,)), ((), ())), preferred_element_type=jnp.float32)


def hidden_units(rows, gate_ups):
    parts = []
    for gate_up in gate_ups:
        both = dot(rows, gate_up)
        n = both.shape[1] // 2
        parts.append((jax.nn.silu(both[:, :n]) * both[:, n:]).astype(jnp.bfloat16))
    return jnp.concatenate(parts, axis=1)


def down(hidden, downs):
    total, at = None, 0
    for weights in downs:
        n = weights.shape[1]
        part = dot_t(hidden[:, at : at + n], weights)
        total, at = part if total is None else total + part, at + n
    return total


def feed(normed, gate_ups, downs, together):
    length = normed.shape[0]
    if together:
        hidden = hidden_units(jnp.concatenate([normed, other(normed)], axis=0), gate_ups)
        mine, others = hidden[:length], hidden[length:]
    else:
        mine, others = (hidden_units(x, gate_ups) for x in (normed, other(normed)))
    received = other(down(others, downs).astype(jnp.bfloat16))
    return down(mine, downs) + received.astype(jnp.float32)


def causal_taps(padded, kernel, length):
    output = jnp.zeros((length, padded.shape[1]), jnp.float32)
    for tap_index in range(kernel.shape[0]):
        output = output + padded[tap_index : tap_index + length] * kernel[tap_index]
    return output


def shards(
    tokens,
    norm_first,
    norm_mixer,
    norm_second,
    ffn_gate,
    ffn_up,
    ffn_down,
    conv_value,
    conv_gate,
    depthwise,
    conv_gain,
    conv_out,
):
    width = tokens.shape[-1]
    tp = lax.axis_index("tp")
    coords = jnp.stack([lax.axis_index(a) for a in ("x", "y", ("zh", "zl"), "tp")]).astype(jnp.int32)
    c = conv_value.shape[1]
    wide, narrow = packed(coords, ffn_gate, ffn_up, ffn_down.T, conv_value, conv_gate, conv_out.T)
    gate_ups, (down_wide, value_gate, out_half, down_narrow) = gathered(coords, wide, narrow)
    downs = (down_wide, down_narrow)
    value_gate_o = other(value_gate)
    out_half_o = other(out_half)
    taps = jnp.concatenate([depthwise, conv_gain[None, :]], axis=0).astype(jnp.float32)
    taps_o = other(taps)

    stream = tokens.reshape(-1, width).astype(jnp.float32)
    length = stream.shape[0]
    stream = stream + 0.5 * feed(rms_rows(stream, norm_first), gate_ups, downs, True)

    normed = rms_rows(stream, norm_mixer)
    both, both_o = dot(normed, value_gate), dot(normed, value_gate_o)
    glu = jnp.concatenate(
        [both[:, :c] * jax.nn.sigmoid(both[:, c:]), both_o[:, :c] * jax.nn.sigmoid(both_o[:, c:])],
        axis=1,
    )
    kernel = jnp.concatenate([taps, taps_o], axis=1)
    reach = depthwise.shape[0] - 1
    tail = glu[length - reach :]
    swapped = jnp.concatenate([tail[:, c:], tail[:, :c]], axis=1)
    before = jnp.where(tp == 1, other(swapped), 0.0)
    conv = causal_taps(jnp.concatenate([before, glu], axis=0), kernel[:-1], length)
    average = jnp.mean(conv, axis=1, keepdims=True)
    centred = conv - average
    spread = jnp.mean(centred * centred, axis=1, keepdims=True)
    activated = jax.nn.silu(centred * lax.rsqrt(spread + CHAN_EPS) * kernel[-1]).astype(jnp.bfloat16)
    stream = stream + dot_t(activated[:, :c], out_half) + dot_t(activated[:, c:], out_half_o)

    stream = stream + 0.5 * feed(rms_rows(stream, norm_second), gate_ups, downs, False)
    return stream.astype(jnp.bfloat16).reshape(tokens.shape)


def solution(mesh):
    mesh = Mesh(mesh.devices.reshape(2, 2, 4, 4, 2), ("zh", "zl", "y", "x", "tp"))
    seqs, rows = ("zh", "zl", "y", "x"), ("zl", "y", "x")
    in_specs = (
        P(seqs, "tp", None),
        P(),
        P(),
        P(),
        P(rows, "tp"),
        P(rows, "tp"),
        P("tp", rows),
        P(rows, "tp"),
        P(rows, "tp"),
        P(None, "tp"),
        P("tp"),
        P("tp", rows),
    )
    out_specs = P(seqs, "tp", None)
    return jax.shard_map(shards, mesh=mesh, in_specs=in_specs, out_specs=out_specs, check_vma=False)
```

time: 199 us -> 165 us (0.83)
  waiting for transfers between devices: 125 us -> 81.1 us
  starting transfers between devices: 3.58 us -> 32.5 us
  between operations: 13.8 us -> 0.62 us
  matrix products: 43.7 us -> 32.6 us
  Pallas kernels: 0 us -> 9.44 us
  local copies, waits for them, and re-layouts: 5 us -> 1.85 us
    all_gather x1 -> x0, waiting for transfers between devices: 115 us -> none  [shards(): full = lax.all_gather(mine, ('rep', 'fs'), axis=0, tiled=True)]
    ppermute x0 -> x22, waiting for transfers between devices: none -> 75.7 us  [from_ring(): return lax.ppermute(x, ALL, pairs)]
    ppermute x0 -> x22, starting transfers between devices: none -> 22.5 us  [from_ring(): return lax.ppermute(x, ALL, pairs)]
    pallas_call x0 -> x5, Pallas kernels: none -> 9.44 us  [copied(): pl.pallas_call(body, in_specs=[SMEM] + [ANY] * count, out_specs=[ANY] * l...]
    ppermute x8, starting transfers between devices: 3.58 us -> 9.98 us  [other(): return lax.ppermute(x, 'tp', SWAP)]
    dot_general x6 -> x8, matrix products: 23.6 us -> 17.7 us  [dot(): return jnp.dot(a, b, preferred_element_type=jnp.float32)]
    dot_general x10, matrix products: 20.1 us -> 14.9 us  [dot_t(): lax.dot_general(a, b, (((1,), (1,)), ((), ())), preferred_element_type=jn...]
    slice x4 -> x0, local copies, waits for them, and re-layouts: 4.93 us -> none  [the longest x1 1.75 us: shards(): value_gate = first[:, n:n + 2 * c]]
  transfers between devices with their start and end apart: 9 -> 30, of which waited for: 5 -> 15; matrix products, arithmetic and copies ran while one was open for 9% -> 10% of each run, Pallas kernels for 0% -> 3%
where the time goes in v2:
time: 165 us; the launch traced here: 164 us
  waiting for transfers between devices  81.1 us (49%)
  matrix products  32.6 us (20%)
  starting transfers between devices  32.5 us (20%)
  Pallas kernels  9.44 us (6%)
  other arithmetic  6.05 us (4%)
  local copies, waits for them, and re-layouts  1.85 us (1%)
    ppermute x22, waiting for transfers between devices, from_ring(): return lax.ppermute(x, ALL, pairs)  75.7 us
    ppermute x22, starting transfers between devices, from_ring(): return lax.ppermute(x, ALL, pairs)  22.5 us
    dot_general x8, matrix products, dot(): return jnp.dot(a, b, preferred_element_type=jnp.float32)  17.7 us
    dot_general x10, matrix products, dot_t(): lax.dot_general(a, b, (((1,), (1,)), ((), ())), preferred_element_type=jn...  14.9 us
    ppermute x8, starting transfers between devices, other(): return lax.ppermute(x, 'tp', SWAP)  9.98 us
    pallas_call x5, Pallas kernels, copied(): pl.pallas_call(body, in_specs=[SMEM] + [ANY] * count, out_specs=[ANY] * l...  9.44 us
    ppermute x8, waiting for transfers between devices, other(): return lax.ppermute(x, 'tp', SWAP)  5.44 us
  transfers between devices with their start and end apart: 30, of which 15 were waited for; matrix products, arithmetic and copies ran while one was open for 10% of the time, Pallas kernels for 3%

profile of v2, /device:TPU:3, one launch (start us, length us, event | category | flops | bytes accessed | tf_op | source)
XLA Modules:
  0.0 164.1 jit_solution(1937094556419527041)
XLA Ops:
  0.1 1.7 %shard_map.118 = (bf16[32,3328]{1,0:T(8,128)(2,1)S(1)}, bf16[64,1664]{1,0:T(8,128)(2,1)S(1)}) custom-call(s32[4]{0:T(128)S(1)} %pad_add_fusion.coords_ref, bf16[64,1408]{1,0:T(8,128)(2,1)} %refs_0_.1, bf16[64,1408]{1,0:T(8,128)(2,1)} %refs_1_.1, bf16[64,1408]{1,0:T(8,128)(2,1)} %bitcast.91, bf16[64,256]{1,0:T(8,128)(2,1)} %refs_3_.1, ...), custom_call_target="tpu_custom_call" | custom-call | tf_op jit(solution)/shard_map/pallas_call | solution.py:61
  1.8 2.8 %collective-permute-start.1 = (bf16[32,3328]{1,0:T(8,128)(2,1)S(1)}, bf16[32,3328]{1,0:T(8,128)(2,1)S(1)}, u32[]{:S(2)}, u32[]{:S(2)}) collective-permute-start(bf16[32,3328]{1,0:T(8,128)(2,1)S(1)} %get-tuple-element.35.refs_0_), channel_id=1, source_target_pairs={{2,0},{9,1},{4,2},{11,3},{6,4},{13,5},{0,6},{15,7},{10,8},{17,9},{... | collective-permute-start | bytes 638984 | tf_op jit(solution)/shard_map/ppermute | solution.py:34
  7.2 2.4 %collective-permute-done.1.refs_1_ = bf16[32,3328]{1,0:T(8,128)(2,1)S(1)} collective-permute-done((bf16[32,3328]{1,0:T(8,128)(2,1)S(1)}, bf16[32,3328]{1,0:T(8,128)(2,1)S(1)}, u32[]{:S(2)}, u32[]{:S(2)}) %collective-permute-start.1) | collective-permute-done | bytes 213024 | tf_op jit(solution)/shard_map/ppermute | solution.py:34
  10.9 2.2 %collective-permute-done.3.refs_3_ = bf16[32,3328]{1,0:T(8,128)(2,1)S(1)} collective-permute-done((bf16[32,3328]{1,0:T(8,128)(2,1)S(1)}, bf16[32,3328]{1,0:T(8,128)(2,1)S(1)}, u32[]{:S(2)}, u32[]{:S(2)}) %collective-permute-start.3) | collective-permute-done | bytes 213024 | tf_op jit(solution)/shard_map/ppermute | solution.py:34
  13.0 2.2 %shard_map.119 = (bf16[4,32,3328]{2,1,0:T(8,128)(2,1)S(1)}, bf16[2,64,1664]{2,1,0:T(8,128)(2,1)S(1)}) custom-call(s32[4]{0:T(128)S(1)} %pad_add_fusion.coords_ref, bf16[32,3328]{1,0:T(8,128)(2,1)S(1)} %get-tuple-element.35.refs_0_, bf16[32,3328]{1,0:T(8,128)(2,1)S(1)} %collective-permute-done.1.refs_1_, bf16[32,3328]{1,0:T(8,128)(2,1)S(1)} %collective-permute-done.2.refs_2_, ...), custom_call_target="tpu_custom_call" | custom-call | tf_op jit(solution)/shard_map/pallas_call | solution.py:61
  16.6 3.8 %collective-permute-start.5 = (bf16[4,32,3328]{2,1,0:T(8,128)(2,1)S(1)}, bf16[4,32,3328]{2,1,0:T(8,128)(2,1)S(1)}, u32[]{:S(2)}, u32[]{:S(2)}) collective-permute-start(bf16[4,32,3328]{2,1,0:T(8,128)(2,1)S(1)} %get-tuple-element.43.refs_0_), channel_id=1, source_target_pairs={{8,0},{33,1},{10,2},{35,3},{12,4},{37,5},{14,6},{39,7},{16,8},{41,... | collective-permute-start | bytes 2555912 | tf_op jit(solution)/shard_map/ppermute | solution.py:34
  21.5 4.2 %collective-permute-done.10.refs_7_ = bf16[2,64,1664]{2,1,0:T(8,128)(2,1)S(1)} collective-permute-done((bf16[2,64,1664]{2,1,0:T(8,128)(2,1)S(1)}, bf16[2,64,1664]{2,1,0:T(8,128)(2,1)S(1)}, u32[]{:S(2)}, u32[]{:S(2)}) %collective-permute-start.10) | collective-permute-done | bytes 426016 | tf_op jit(solution)/shard_map/ppermute | solution.py:34
  25.6 2.1 %collective-permute-start.9 = (bf16[2,64,1664]{2,1,0:T(8,128)(2,1)S(1)}, bf16[2,64,1664]{2,1,0:T(8,128)(2,1)S(1)}, u32[]{:S(2)}, u32[]{:S(2)}) collective-permute-start(bf16[2,64,1664]{2,1,0:T(8,128)(2,1)S(1)} %get-tuple-element.47.refs_4_), channel_id=1, source_target_pairs={{4,0},{5,1},{6,2},{7,3},{0,4},{1,5},{2,6},{3,7},{12,8},{13,9},{14,... | collective-permute-start | bytes 1277960 | tf_op jit(solution)/shard_map/ppermute | solution.py:34
  27.7 4.1 %collective-permute-done.8.refs_5_ = bf16[2,64,1664]{2,1,0:T(8,128)(2,1)S(1)} collective-permute-done((bf16[2,64,1664]{2,1,0:T(8,128)(2,1)S(1)}, bf16[2,64,1664]{2,1,0:T(8,128)(2,1)S(1)}, u32[]{:S(2)}, u32[]{:S(2)}) %collective-permute-start.8) | collective-permute-done | bytes 426016 | tf_op jit(solution)/shard_map/ppermute | solution.py:34
  31.8 9.2 %collective-permute-done.9.refs_6_ = bf16[2,64,1664]{2,1,0:T(8,128)(2,1)S(1)} collective-permute-done((bf16[2,64,1664]{2,1,0:T(8,128)(2,1)S(1)}, bf16[2,64,1664]{2,1,0:T(8,128)(2,1)S(1)}, u32[]{:S(2)}, u32[]{:S(2)}) %collective-permute-start.9) | collective-permute-done | bytes 426016 | tf_op jit(solution)/shard_map/ppermute | solution.py:34
  48.3 7.9 %collective-permute-done.20.refs_5_ = bf16[4,2,64,640]{3,2,1,0:T(8,128)(2,1)S(1)} collective-permute-done((bf16[4,2,64,640]{3,2,1,0:T(8,128)(2,1)S(1)}, bf16[4,2,64,640]{3,2,1,0:T(8,128)(2,1)S(1)}, u32[]{:S(2)}, u32[]{:S(2)}) %collective-permute-start.20) | collective-permute-done | bytes 655392 | tf_op jit(solution)/shard_map/ppermute | solution.py:34
  56.2 7.0 %collective-permute-done.17.refs_1_ = bf16[4,4,32,1536]{3,2,1,0:T(8,128)(2,1)S(1)} collective-permute-done((bf16[4,4,32,1536]{3,2,1,0:T(8,128)(2,1)S(1)}, bf16[4,4,32,1536]{3,2,1,0:T(8,128)(2,1)S(1)}, u32[]{:S(2)}, u32[]{:S(2)}) %collective-permute-start.17) | collective-permute-done | bytes 1572896 | tf_op jit(solution)/shard_map/ppermute | solution.py:34
  64.3 12.1 %collective-permute-done.22.refs_7_ = bf16[4,2,64,640]{3,2,1,0:T(8,128)(2,1)S(1)} collective-permute-done((bf16[4,2,64,640]{3,2,1,0:T(8,128)(2,1)S(1)}, bf16[4,2,64,640]{3,2,1,0:T(8,128)(2,1)S(1)}, u32[]{:S(2)}, u32[]{:S(2)}) %collective-permute-start.22) | collective-permute-done | bytes 655392 | tf_op jit(solution)/shard_map/ppermute | solution.py:34
  78.2 7.9 %collective-permute-done.21.refs_6_ = bf16[4,2,64,640]{3,2,1,0:T(8,128)(2,1)S(1)} collective-permute-done((bf16[4,2,64,640]{3,2,1,0:T(8,128)(2,1)S(1)}, bf16[4,2,64,640]{3,2,1,0:T(8,128)(2,1)S(1)}, u32[]{:S(2)}, u32[]{:S(2)}) %collective-permute-start.21) | collective-permute-done | bytes 655392 | tf_op jit(solution)/shard_map/ppermute | solution.py:34
  87.9 5.2 %collective-permute-start = (bf16[256,2048]{1,0:T(8,128)(2,1)S(1)}, bf16[256,2048]{1,0:T(8,128)(2,1)S(1)}, u32[]{:S(2)}, u32[]{:S(2)}) collective-permute-start(bf16[256,2048]{1,0:T(8,128)(2,1)S(1)} %fusion.12), channel_id=1, source_target_pairs={{0,1},{1,0},{2,3},{3,2},{4,5},{5,4},{6,7},{7,6},{8,9},{9,8},{10,11... | collective-permute-start | bytes 3145736 | tf_op jit(solution)/shard_map/ppermute | solution.py:21
  93.1 1.9 %shard_map.122 = (bf16[2,4,4,2,32,768]{5,4,3,2,1,0:T(8,128)(2,1)S(1)}, bf16[2,4,4,2,32,512]{5,4,3,2,1,0:T(8,128)(2,1)}, bf16[2,4,4,2,32,256]{5,4,3,2,1,0:T(8,128)(2,1)S(1)}, bf16[2,4,4,64,640]{4,3,2,1,0:T(8,128)(2,1)S(1)}) custom-call(s32[4]{0:T(128)S(1)} %pad_add_fusion.coords_ref, bf16[4,4,32,1536]{3,2,1,0:T(8,128)(2,1)S(1)} %get-tuple-element.54.refs_0_, ...), custom_call_target="tpu_custom_call" | custom-call | tf_op jit(solution)/shard_map/pallas_call | solution.py:61
  95.1 12.3 %collective-permute-done.16.refs_7_ = bf16[4,2,64,1024]{3,2,1,0:T(8,128)(2,1)S(1)} collective-permute-done((bf16[4,2,64,1024]{3,2,1,0:T(8,128)(2,1)S(1)}, bf16[4,2,64,1024]{3,2,1,0:T(8,128)(2,1)S(1)}, u32[]{:S(2)}, u32[]{:S(2)}) %collective-permute-start.16) | collective-permute-done | bytes 1048608 | tf_op jit(solution)/shard_map/ppermute | solution.py:34
  107.4 3.7 %collective-permute-done.15.refs_6_ = bf16[4,2,64,1024]{3,2,1,0:T(8,128)(2,1)S(1)} collective-permute-done((bf16[4,2,64,1024]{3,2,1,0:T(8,128)(2,1)S(1)}, bf16[4,2,64,1024]{3,2,1,0:T(8,128)(2,1)S(1)}, u32[]{:S(2)}, u32[]{:S(2)}) %collective-permute-start.15) | collective-permute-done | bytes 1048608 | tf_op jit(solution)/shard_map/ppermute | solution.py:34
  111.1 2.6 %shard_map.121 = (bf16[2,4,4,2,32,1792]{5,4,3,2,1,0:T(8,128)(2,1)S(1)}, bf16[2,4,4,64,1024]{4,3,2,1,0:T(8,128)(2,1)S(1)}) custom-call(s32[4]{0:T(128)S(1)} %pad_add_fusion.coords_ref, bf16[4,4,32,1792]{3,2,1,0:T(8,128)(2,1)S(1)} %get-tuple-element.51.refs_0_, bf16[4,4,32,1792]{3,2,1,0:T(8,128)(2,1)S(1)} %collective-permute-done.11.refs_1_, ...), custom_call_target="tpu_custom_call" | custom-call | tf_op jit(solution)/shard_map/pallas_call | solution.py:61
  113.7 3.9 %fusion.15 = f32[512,1792]{1,0:T(8,128)S(1)} fusion(bf16[2048,1792]{1,0:T(8,128)(2,1)S(1)} %bitcast.83, bf16[256,2048]{1,0:T(8,128)(2,1)S(1)} %collective-permute-done, bf16[256,2048]{1,0:T(8,128)(2,1)S(1)} %fusion.12), kind=kOutput, calls=%fused_computation.29 | convolution fusion | flops 3762290688 | bytes 13107200 | tf_op jit(solution)/shard_map/dot_general | solution.py:216
  118.2 2.3 %fusion.14 = f32[512,1024]{1,0:T(8,128)S(1)} fusion(bf16[2048,1024]{1,0:T(8,128)(2,1)S(1)} %bitcast.88, bf16[256,2048]{1,0:T(8,128)(2,1)S(1)} %collective-permute-done, bf16[256,2048]{1,0:T(8,128)(2,1)S(1)} %fusion.12), kind=kOutput, calls=%fused_computation.28 | convolution fusion | flops 2151677952 | bytes 8388608 | tf_op jit(solution)/shard_map/dot_general | solution.py:216
  122.0 2.1 %fusion.7 = bf16[256,2048]{1,0:T(8,128)(2,1)} fusion(f32[256,2048]{1,0:T(8,128)S(1)} %fusion.59, bf16[2048,768]{1,0:T(8,128)(2,1)S(1)} %bitcast.73, bf16[512,896]{1,0:T(8,128)(2,1)S(1)} %fusion.13), kind=kOutput, calls=%fused_computation.15 | convolution fusion | flops 806354944 | bytes 6684672 | tf_op jit(solution)/shard_map/dot_general | solution.py:220
  124.0 2.1 %collective-permute-start.23 = (bf16[256,2048]{1,0:T(8,128)(2,1)}, bf16[256,2048]{1,0:T(8,128)(2,1)}, u32[]{:S(2)}, u32[]{:S(2)}) collective-permute-start(bf16[256,2048]{1,0:T(8,128)(2,1)} %fusion.7), channel_id=1, source_target_pairs={{0,1},{1,0},{2,3},{3,2},{4,5},{5,4},{6,7},{7,6},{8,9},{9,8},{10,11... | collective-permute-start | bytes 3145736 | tf_op jit(solution)/shard_map/ppermute | solution.py:21
  126.8 5.0 %collective-permute-done.26 = f32[32,256]{1,0:T(8,128)S(1)} collective-permute-done((f32[32,256]{1,0:T(8,128)S(1)}, f32[32,256]{1,0:T(8,128)S(1)}, u32[]{:S(2)}, u32[]{:S(2)}) %collective-permute-start.26) | collective-permute-done | bytes 32800 | tf_op jit(solution)/shard_map/ppermute | solution.py:21
  131.9 2.9 %fusion.61 = f32[256,2048]{1,0:T(8,128)S(1)} fusion(bf16[2048,640]{1,0:T(8,128)(2,1)} %bitcast.78, bf16[512,512]{1,0:T(8,128)(2,1)} %copy-done.10, bf16[512,896]{1,0:T(8,128)(2,1)} %copy-done.7), kind=kOutput, calls=%fused_computation.179 | convolution fusion | flops 671744000 | bytes 6160384 | tf_op jit(solution)/shard_map/dot_general | solution.py:220
  134.9 2.6 %multiply_reduce_fusion.1 = (f32[256]{0:T(256)S(1)}, f32[256,2048]{1,0:T(8,128)S(1)}) fusion(bf16[256,2048]{1,0:T(8,128)(2,1)} %collective-permute-done.23, f32[256,2048]{1,0:T(8,128)S(1)} %fusion.61, bf16[2048,768]{1,0:T(8,128)(2,1)S(1)} %bitcast.74, bf16[512,896]{1,0:T(8,128)(2,1)} %copy-done.7, bf16[1,256,2048]{2,1,0:T(8,128)(2,1)S(1)} %copy-done.9), kind=kOutput, calls=%fused_computation.25 | convolution fusion | flops 809500416 | bytes 9831424 | tf_op jit(solution)/shard_map/dot_general | solution.py:220
  137.5 2.4 %fusion.113 = f32[256,512]{1,0:T(8,128)S(1)} fusion(bf16[2048,512]{1,0:T(8,128)(2,1)} %bitcast.12, f32[256,2048]{1,0:T(8,128)S(1)} %get-tuple-element.96, f32[2048]{0:T(1024)S(1)} %convert_element_type.71, f32[256]{0:T(256)S(1)} %add_rsqrt_fusion.2), kind=kOutput, calls=%fused_computation.243 | convolution fusion | flops 538443776 | bytes 4727808 | tf_op jit(solution)/shard_map/dot_general | solution.py:216
  140.0 2.4 %fusion.114 = f32[256,512]{1,0:T(8,128)S(1)} fusion(bf16[2048,512]{1,0:T(8,128)(2,1)} %collective-permute-done.24, f32[256,2048]{1,0:T(8,128)S(1)} %get-tuple-element.96, f32[2048]{0:T(1024)S(1)} %convert_element_type.71, f32[256]{0:T(256)S(1)} %add_rsqrt_fusion.2), kind=kOutput, calls=%fused_computation.244 | convolution fusion | flops 538443776 | bytes 4727808 | tf_op jit(solution)/shard_map/dot_general | solution.py:216
  143.9 2.6 %fusion.115 = (f32[256]{0:T(256)S(1)}, f32[256,512]{1,0:T(8,128)S(1)}) fusion(f32[512]{0:T(512)S(1)} %bitcast.97, f32[256,256]{1,0:T(8,128)S(1)} %fusion.72, f32[256,256]{1,0:T(8,128)S(1)} %fusion.68, f32[512]{0:T(512)S(1)} %bitcast.96, f32[286,512]{1,0:T(8,128)S(1)} %maximum_maximum_fusion, f32[512]{0:T(512)S(1)} %bitcast.95, f32[512]{0:T(512)S(1)} %bitcast.94, ...), kind=kLoop, calls=%fused_computation.245 | loop fusion | flops 8257280 | bytes 16841728 | tf_op jit(solution)/shard_map/reduce_sum | solution.py:301
  150.3 2.1 %fusion.117 = f32[256,1792]{1,0:T(8,128)S(1)} fusion(bf16[256,2048]{1,0:T(8,128)(2,1)S(1)} %multiply_convert_fusion, bf16[2048,1792]{1,0:T(8,128)(2,1)S(1)} %bitcast.86), kind=kOutput, calls=%fused_computation.246 | convolution fusion | flops 1879048192 | bytes 10223616 | tf_op jit(solution)/shard_map/dot_general | solution.py:216
  152.4 2.1 %fusion.119 = f32[256,1792]{1,0:T(8,128)S(1)} fusion(bf16[256,2048]{1,0:T(8,128)(2,1)S(1)} %collective-permute-done.28, bf16[2048,1792]{1,0:T(8,128)(2,1)S(1)} %bitcast.87), kind=kOutput, calls=%fused_computation.248 | convolution fusion | flops 1879048192 | bytes 10223616 | tf_op jit(solution)/shard_map/dot_general | solution.py:216
  162.1 2.1 %fusion.9 = bf16[1,256,2048]{2,1,0:T(8,128)(2,1)} fusion(f32[256,2048]{1,0:T(8,128)S(1)} %get-tuple-element.98, f32[256,2048]{1,0:T(8,128)S(1)} %fusion.57, bf16[2048,768]{1,0:T(8,128)(2,1)S(1)} %bitcast.76, bf16[256,2048]{1,0:T(8,128)(2,1)S(1)} %collective-permute-done.29, bf16[256,896]{1,0:T(8,128)(2,1)S(1)} %fusion.18), kind=kOutput, calls=%fused_computation.17 | convolution fusion | flops 808452096 | bytes 9830400 | tf_op jit(solution)/shard_map/dot_general | solution.py:220
  (122 shorter events, 33.7 us)
Async XLA Ops:
  1.8 7.9 %collective-permute-start.1 = (bf16[32,3328]{1,0:T(8,128)(2,1)S(1)}, bf16[32,3328]{1,0:T(8,128)(2,1)S(1)}, u32[]{:S(2)}, u32[]{:S(2)}) collective-permute-start(bf16[32,3328]{1,0:T(8,128)(2,1)S(1)} %get-tuple-element.35.refs_0_), channel_id=1, source_target_pairs={{2,0},{9,1},{4,2},{11,3},{6,4},{13,5},{0,6},{15,7},{10,8},{17,9},{... | collective-permute-start | bytes 638984 | tf_op jit(solution)/shard_map/ppermute | solution.py:34
  4.6 6.3 %collective-permute-start.2 = (bf16[32,3328]{1,0:T(8,128)(2,1)S(1)}, bf16[32,3328]{1,0:T(8,128)(2,1)S(1)}, u32[]{:S(2)}, u32[]{:S(2)}) collective-permute-start(bf16[32,3328]{1,0:T(8,128)(2,1)S(1)} %get-tuple-element.35.refs_0_), channel_id=1, source_target_pairs={{4,0},{17,1},{6,2},{19,3},{0,4},{21,5},{2,6},{23,7},{12,8},{25,9},... | collective-permute-start | bytes 638984 | tf_op jit(solution)/shard_map/ppermute | solution.py:34
  4.9 8.1 %collective-permute-start.3 = (bf16[32,3328]{1,0:T(8,128)(2,1)S(1)}, bf16[32,3328]{1,0:T(8,128)(2,1)S(1)}, u32[]{:S(2)}, u32[]{:S(2)}) collective-permute-start(bf16[32,3328]{1,0:T(8,128)(2,1)S(1)} %get-tuple-element.35.refs_0_), channel_id=1, source_target_pairs={{6,0},{25,1},{0,2},{27,3},{2,4},{29,5},{4,6},{31,7},{14,8},{1,9},{... | collective-permute-start | bytes 638984 | tf_op jit(solution)/shard_map/ppermute | solution.py:34
  5.6 7.4 %collective-permute-start.4 = (bf16[64,1664]{1,0:T(8,128)(2,1)S(1)}, bf16[64,1664]{1,0:T(8,128)(2,1)S(1)}, u32[]{:S(2)}, u32[]{:S(2)}) collective-permute-start(bf16[64,1664]{1,0:T(8,128)(2,1)S(1)} %get-tuple-element.39.refs_4_), channel_id=1, source_target_pairs={{32,0},{97,1},{34,2},{99,3},{36,4},{101,5},{38,6},{103,7},{40,8},{... | collective-permute-start | bytes 638984 | tf_op jit(solution)/shard_map/ppermute | solution.py:34
  15.3 10.3 %collective-permute-start.10 = (bf16[2,64,1664]{2,1,0:T(8,128)(2,1)S(1)}, bf16[2,64,1664]{2,1,0:T(8,128)(2,1)S(1)}, u32[]{:S(2)}, u32[]{:S(2)}) collective-permute-start(bf16[2,64,1664]{2,1,0:T(8,128)(2,1)S(1)} %get-tuple-element.47.refs_4_), channel_id=1, source_target_pairs={{6,0},{7,1},{0,2},{1,3},{2,4},{3,5},{4,6},{5,7},{14,8},{15,9},{8,1... | collective-permute-start | bytes 1277960 | tf_op jit(solution)/shard_map/ppermute | solution.py:34
  16.6 61.3 %copy-start.8 = (bf16[1,256,2048]{2,1,0:T(8,128)(2,1)S(1)}, bf16[1,256,2048]{2,1,0:T(8,128)(2,1)}, u32[]{:S(2)}) copy-start(bf16[1,256,2048]{2,1,0:T(8,128)(2,1)} %param.12) | copy-start | bytes 3145732
  16.6 61.6 %copy-start.12 = (bf16[2048]{0:T(1024)(128)(2,1)S(1)}, bf16[2048]{0:T(1024)(128)(2,1)}, u32[]{:S(2)}) copy-start(bf16[2048]{0:T(1024)(128)(2,1)} %param.13) | copy-start | bytes 12292
  16.6 24.3 %collective-permute-start.5 = (bf16[4,32,3328]{2,1,0:T(8,128)(2,1)S(1)}, bf16[4,32,3328]{2,1,0:T(8,128)(2,1)S(1)}, u32[]{:S(2)}, u32[]{:S(2)}) collective-permute-start(bf16[4,32,3328]{2,1,0:T(8,128)(2,1)S(1)} %get-tuple-element.43.refs_0_), channel_id=1, source_target_pairs={{8,0},{33,1},{10,2},{35,3},{12,4},{37,5},{14,6},{39,7},{16,8},{41,... | collective-permute-start | bytes 2555912 | tf_op jit(solution)/shard_map/ppermute | solution.py:34
  20.3 20.6 %collective-permute-start.6 = (bf16[4,32,3328]{2,1,0:T(8,128)(2,1)S(1)}, bf16[4,32,3328]{2,1,0:T(8,128)(2,1)S(1)}, u32[]{:S(2)}, u32[]{:S(2)}) collective-permute-start(bf16[4,32,3328]{2,1,0:T(8,128)(2,1)S(1)} %get-tuple-element.43.refs_0_), channel_id=1, source_target_pairs={{16,0},{65,1},{18,2},{67,3},{20,4},{69,5},{22,6},{71,7},{24,8},{73... | collective-permute-start | bytes 2555912 | tf_op jit(solution)/shard_map/ppermute | solution.py:34
  20.3 22.2 %collective-permute-start.7 = (bf16[4,32,3328]{2,1,0:T(8,128)(2,1)S(1)}, bf16[4,32,3328]{2,1,0:T(8,128)(2,1)S(1)}, u32[]{:S(2)}, u32[]{:S(2)}) collective-permute-start(bf16[4,32,3328]{2,1,0:T(8,128)(2,1)S(1)} %get-tuple-element.43.refs_0_), channel_id=1, source_target_pairs={{24,0},{97,1},{26,2},{99,3},{28,4},{101,5},{30,6},{103,7},{0,8},{1... | collective-permute-start | bytes 2555912 | tf_op jit(solution)/shard_map/ppermute | solution.py:34
  21.0 10.7 %collective-permute-start.8 = (bf16[2,64,1664]{2,1,0:T(8,128)(2,1)S(1)}, bf16[2,64,1664]{2,1,0:T(8,128)(2,1)S(1)}, u32[]{:S(2)}, u32[]{:S(2)}) collective-permute-start(bf16[2,64,1664]{2,1,0:T(8,128)(2,1)S(1)} %get-tuple-element.47.refs_4_), channel_id=1, source_target_pairs={{2,0},{3,1},{4,2},{5,3},{6,4},{7,5},{0,6},{1,7},{10,8},{11,9},{12,... | collective-permute-start | bytes 1277960 | tf_op jit(solution)/shard_map/ppermute | solution.py:34
  25.6 15.3 %collective-permute-start.9 = (bf16[2,64,1664]{2,1,0:T(8,128)(2,1)S(1)}, bf16[2,64,1664]{2,1,0:T(8,128)(2,1)S(1)}, u32[]{:S(2)}, u32[]{:S(2)}) collective-permute-start(bf16[2,64,1664]{2,1,0:T(8,128)(2,1)S(1)} %get-tuple-element.47.refs_4_), channel_id=1, source_target_pairs={{4,0},{5,1},{6,2},{7,3},{0,4},{1,5},{2,6},{3,7},{12,8},{13,9},{14,... | collective-permute-start | bytes 1277960 | tf_op jit(solution)/shard_map/ppermute | solution.py:34
  43.6 19.6 %collective-permute-start.17 = (bf16[4,4,32,1536]{3,2,1,0:T(8,128)(2,1)S(1)}, bf16[4,4,32,1536]{3,2,1,0:T(8,128)(2,1)S(1)}, u32[]{:S(2)}, u32[]{:S(2)}) collective-permute-start(bf16[4,4,32,1536]{3,2,1,0:T(8,128)(2,1)S(1)} %get-tuple-element.54.refs_0_), channel_id=1, source_target_pairs={{96,0},{7,1},{98,2},{1,3},{100,4},{3,5},{102,6},{5,7},{104,8},{15,... | collective-permute-start | bytes 4718600 | tf_op jit(solution)/shard_map/ppermute | solution.py:34
  44.7 31.7 %collective-permute-start.11 = (bf16[4,4,32,1792]{3,2,1,0:T(8,128)(2,1)S(1)}, bf16[4,4,32,1792]{3,2,1,0:T(8,128)(2,1)S(1)}, u32[]{:S(2)}, u32[]{:S(2)}) collective-permute-start(bf16[4,4,32,1792]{3,2,1,0:T(8,128)(2,1)S(1)} %get-tuple-element.51.refs_0_), channel_id=1, source_target_pairs={{32,0},{3,1},{34,2},{5,3},{36,4},{7,5},{38,6},{1,7},{40,8},{11,9},... | collective-permute-start | bytes 5505032 | tf_op jit(solution)/shard_map/ppermute | solution.py:34
  45.1 11.1 %collective-permute-start.20 = (bf16[4,2,64,640]{3,2,1,0:T(8,128)(2,1)S(1)}, bf16[4,2,64,640]{3,2,1,0:T(8,128)(2,1)S(1)}, u32[]{:S(2)}, u32[]{:S(2)}) collective-permute-start(bf16[4,2,64,640]{3,2,1,0:T(8,128)(2,1)S(1)} %get-tuple-element.55.refs_4_), channel_id=1, source_target_pairs={{24,0},{9,1},{26,2},{11,3},{28,4},{13,5},{30,6},{15,7},{0,8},{17,9... | collective-permute-start | bytes 1966088 | tf_op jit(solution)/shard_map/ppermute | solution.py:34
  45.6 41.8 %collective-permute-start.19 = (bf16[4,4,32,1536]{3,2,1,0:T(8,128)(2,1)S(1)}, bf16[4,4,32,1536]{3,2,1,0:T(8,128)(2,1)S(1)}, u32[]{:S(2)}, u32[]{:S(2)}) collective-permute-start(bf16[4,4,32,1536]{3,2,1,0:T(8,128)(2,1)S(1)} %get-tuple-element.54.refs_0_), channel_id=1, source_target_pairs={{32,0},{3,1},{34,2},{5,3},{36,4},{7,5},{38,6},{1,7},{40,8},{11,9},... | collective-permute-start | bytes 4718600 | tf_op jit(solution)/shard_map/ppermute | solution.py:34
  47.2 29.2 %collective-permute-start.14 = (bf16[4,2,64,1024]{3,2,1,0:T(8,128)(2,1)S(1)}, bf16[4,2,64,1024]{3,2,1,0:T(8,128)(2,1)S(1)}, u32[]{:S(2)}, u32[]{:S(2)}) collective-permute-start(bf16[4,2,64,1024]{3,2,1,0:T(8,128)(2,1)S(1)} %get-tuple-element.52.refs_4_), channel_id=1, source_target_pairs={{8,0},{25,1},{10,2},{27,3},{12,4},{29,5},{14,6},{31,7},{16,8},{1,9... | collective-permute-start | bytes 3145736 | tf_op jit(solution)/shard_map/ppermute | solution.py:34
  56.2 20.2 %collective-permute-start.22 = (bf16[4,2,64,640]{3,2,1,0:T(8,128)(2,1)S(1)}, bf16[4,2,64,640]{3,2,1,0:T(8,128)(2,1)S(1)}, u32[]{:S(2)}, u32[]{:S(2)}) collective-permute-start(bf16[4,2,64,640]{3,2,1,0:T(8,128)(2,1)S(1)} %get-tuple-element.55.refs_4_), channel_id=1, source_target_pairs={{8,0},{25,1},{10,2},{27,3},{12,4},{29,5},{14,6},{31,7},{16,8},{1,9... | collective-permute-start | bytes 1966088 | tf_op jit(solution)/shard_map/ppermute | solution.py:34
  63.2 24.7 %collective-permute-start.18 = (bf16[4,4,32,1536]{3,2,1,0:T(8,128)(2,1)S(1)}, bf16[4,4,32,1536]{3,2,1,0:T(8,128)(2,1)S(1)}, u32[]{:S(2)}, u32[]{:S(2)}) collective-permute-start(bf16[4,4,32,1536]{3,2,1,0:T(8,128)(2,1)S(1)} %collective-permute-done.17.refs_1_), channel_id=1, source_target_pairs={{96,0},{7,1},{98,2},{1,3},{100,4},{3,5},{102,6},{5,7},{104,8},{15,... | collective-permute-start | bytes 4718600 | tf_op jit(solution)/shard_map/ppermute | solution.py:34
  76.4 9.7 %collective-permute-start.21 = (bf16[4,2,64,640]{3,2,1,0:T(8,128)(2,1)S(1)}, bf16[4,2,64,640]{3,2,1,0:T(8,128)(2,1)S(1)}, u32[]{:S(2)}, u32[]{:S(2)}) collective-permute-start(bf16[4,2,64,640]{3,2,1,0:T(8,128)(2,1)S(1)} %collective-permute-done.20.refs_5_), channel_id=1, source_target_pairs={{24,0},{9,1},{26,2},{11,3},{28,4},{13,5},{30,6},{15,7},{0,8},{17,9... | collective-permute-start | bytes 1966088 | tf_op jit(solution)/shard_map/ppermute | solution.py:34
  76.4 31.0 %collective-permute-start.13 = (bf16[4,4,32,1792]{3,2,1,0:T(8,128)(2,1)S(1)}, bf16[4,4,32,1792]{3,2,1,0:T(8,128)(2,1)S(1)}, u32[]{:S(2)}, u32[]{:S(2)}) collective-permute-start(bf16[4,4,32,1792]{3,2,1,0:T(8,128)(2,1)S(1)} %get-tuple-element.51.refs_0_), channel_id=1, source_target_pairs={{96,0},{7,1},{98,2},{1,3},{100,4},{3,5},{102,6},{5,7},{104,8},{15,... | collective-permute-start | bytes 5505032 | tf_op jit(solution)/shard_map/ppermute | solution.py:34
  76.4 34.7 %collective-permute-start.12 = (bf16[4,4,32,1792]{3,2,1,0:T(8,128)(2,1)S(1)}, bf16[4,4,32,1792]{3,2,1,0:T(8,128)(2,1)S(1)}, u32[]{:S(2)}, u32[]{:S(2)}) collective-permute-start(bf16[4,4,32,1792]{3,2,1,0:T(8,128)(2,1)S(1)} %collective-permute-done.11.refs_1_), channel_id=1, source_target_pairs={{32,0},{3,1},{34,2},{5,3},{36,4},{7,5},{38,6},{1,7},{40,8},{11,9},... | collective-permute-start | bytes 5505032 | tf_op jit(solution)/shard_map/ppermute | solution.py:34
  86.1 21.3 %collective-permute-start.16 = (bf16[4,2,64,1024]{3,2,1,0:T(8,128)(2,1)S(1)}, bf16[4,2,64,1024]{3,2,1,0:T(8,128)(2,1)S(1)}, u32[]{:S(2)}, u32[]{:S(2)}) collective-permute-start(bf16[4,2,64,1024]{3,2,1,0:T(8,128)(2,1)S(1)} %get-tuple-element.52.refs_4_), channel_id=1, source_target_pairs={{24,0},{9,1},{26,2},{11,3},{28,4},{13,5},{30,6},{15,7},{0,8},{17,9... | collective-permute-start | bytes 3145736 | tf_op jit(solution)/shard_map/ppermute | solution.py:34
  87.3 23.8 %collective-permute-start.15 = (bf16[4,2,64,1024]{3,2,1,0:T(8,128)(2,1)S(1)}, bf16[4,2,64,1024]{3,2,1,0:T(8,128)(2,1)S(1)}, u32[]{:S(2)}, u32[]{:S(2)}) collective-permute-start(bf16[4,2,64,1024]{3,2,1,0:T(8,128)(2,1)S(1)} %collective-permute-done.14.refs_5_), channel_id=1, source_target_pairs={{8,0},{25,1},{10,2},{27,3},{12,4},{29,5},{14,6},{31,7},{16,8},{1,9... | collective-permute-start | bytes 3145736 | tf_op jit(solution)/shard_map/ppermute | solution.py:34
  87.9 25.8 %collective-permute-start = (bf16[256,2048]{1,0:T(8,128)(2,1)S(1)}, bf16[256,2048]{1,0:T(8,128)(2,1)S(1)}, u32[]{:S(2)}, u32[]{:S(2)}) collective-permute-start(bf16[256,2048]{1,0:T(8,128)(2,1)S(1)} %fusion.12), channel_id=1, source_target_pairs={{0,1},{1,0},{2,3},{3,2},{4,5},{5,4},{6,7},{7,6},{8,9},{9,8},{10,11... | collective-permute-start | bytes 3145736 | tf_op jit(solution)/shard_map/ppermute | solution.py:21
  124.0 10.8 %collective-permute-start.23 = (bf16[256,2048]{1,0:T(8,128)(2,1)}, bf16[256,2048]{1,0:T(8,128)(2,1)}, u32[]{:S(2)}, u32[]{:S(2)}) collective-permute-start(bf16[256,2048]{1,0:T(8,128)(2,1)} %fusion.7), channel_id=1, source_target_pairs={{0,1},{1,0},{2,3},{3,2},{4,5},{5,4},{6,7},{7,6},{8,9},{9,8},{10,11... | collective-permute-start | bytes 3145736 | tf_op jit(solution)/shard_map/ppermute | solution.py:21
  126.2 13.8 %collective-permute-start.24 = (bf16[2048,512]{1,0:T(8,128)(2,1)}, bf16[2048,512]{1,0:T(8,128)(2,1)}, u32[]{:S(2)}, u32[]{:S(2)}) collective-permute-start(bf16[2048,512]{1,0:T(8,128)(2,1)} %bitcast.12), channel_id=1, source_target_pairs={{0,1},{1,0},{2,3},{3,2},{4,5},{5,4},{6,7},{7,6},{8,9},{9,8},{10,11... | collective-permute-start | bytes 6291464 | tf_op jit(solution)/shard_map/ppermute | solution.py:21
  126.3 5.5 %collective-permute-start.26 = (f32[32,256]{1,0:T(8,128)S(1)}, f32[32,256]{1,0:T(8,128)S(1)}, u32[]{:S(2)}, u32[]{:S(2)}) collective-permute-start(f32[32,256]{1,0:T(8,128)S(1)} %maximum_convert_fusion), channel_id=1, source_target_pairs={{0,1},{1,0},{2,3},{3,2},{4,5},{5,4},{6,7},{7,6},{8,9},{9,8},{10,11... | collective-permute-start | bytes 98312 | tf_op jit(solution)/shard_map/ppermute | solution.py:21
  142.5 1.3 collective-permute-start.25
  143.0 4.1 %collective-permute-start.27 = (bf16[2048,256]{1,0:T(8,128)(2,1)S(1)}, bf16[2048,256]{1,0:T(8,128)(2,1)S(1)}, u32[]{:S(2)}, u32[]{:S(2)}) collective-permute-start(bf16[2048,256]{1,0:T(8,128)(2,1)S(1)} %bitcast.81), channel_id=1, source_target_pairs={{0,1},{1,0},{2,3},{3,2},{4,5},{5,4},{6,7},{7,6},{8,9},{9,8},{10,11... | collective-permute-start | bytes 3145736 | tf_op jit(solution)/shard_map/ppermute | solution.py:21
  148.5 3.9 %collective-permute-start.28 = (bf16[256,2048]{1,0:T(8,128)(2,1)S(1)}, bf16[256,2048]{1,0:T(8,128)(2,1)S(1)}, u32[]{:S(2)}, u32[]{:S(2)}) collective-permute-start(bf16[256,2048]{1,0:T(8,128)(2,1)S(1)} %multiply_convert_fusion), channel_id=1, source_target_pairs={{0,1},{1,0},{2,3},{3,2},{4,5},{5,4},{6,7},{7,6},{8,9},{9,8},{10,11... | collective-permute-start | bytes 3145736 | tf_op jit(solution)/shard_map/ppermute | solution.py:21
  158.6 3.4 %collective-permute-start.29 = (bf16[256,2048]{1,0:T(8,128)(2,1)S(1)}, bf16[256,2048]{1,0:T(8,128)(2,1)S(1)}, u32[]{:S(2)}, u32[]{:S(2)}) collective-permute-start(bf16[256,2048]{1,0:T(8,128)(2,1)S(1)} %fusion.8), channel_id=1, source_target_pairs={{0,1},{1,0},{2,3},{3,2},{4,5},{5,4},{6,7},{7,6},{8,9},{9,8},{10,11... | collective-permute-start | bytes 3145736 | tf_op jit(solution)/shard_map/ppermute | solution.py:21
  (16 other events, 91.0 us)
